TPU v7x, 32 devices: a whole 2x2x4 slice. The times are simulated.
32 devices in a mesh: sp: 8 (over z, y), tp: 4 (over x, core).
Axes of the slice: x: 2, y: 2, z: 4, core: 2. Of those that a mesh axis runs over, the one named last changes fastest.
Arguments:
- tokens: bfloat16 [1536, 2048], P('sp'), may hold values from -10 to 10
- w_query: bfloat16 [2048, 1024], P(None, 'tp'), may hold values from -0.125 to 0.125
- w_key: bfloat16 [2048, 256], P(None, 'tp'), may hold values from -0.125 to 0.125
- w_value: bfloat16 [2048, 256], P(None, 'tp'), may hold values from -0.125 to 0.125
- w_output: bfloat16 [1024, 2048], P('tp'), may hold values from -0.1875 to 0.1875
- query_gain: float32 [64], replicated, may hold values from 0.4 to 9
- key_gain: float32 [64], replicated, may hold values from 0.4 to 9
Outputs:
- mixed_out: bfloat16 [1536, 2048], P(('sp', 'tp'))
- log_sums: float32 [16, 1536], P('tp', 'sp')
All inputs are finite; a program needn't handle non-finite values.
Results may differ from a plain program's by a relative error of at most 0.009.
The roundings to bfloat16 on the way count: a program that leaves them out, or rounds other values in their place, can miss the bound.
Values may be sent and summed in bfloat16 or wider, within the bound.
No kernel may reach another device: no remote copies, remote signals or barrier semaphores. Data moves between devices by JAX's collectives and lax.ppermute only.
A program may use at most 64 MiB of HBM per device.

v0:
```python
import functools

import jax
import jax.numpy as jnp
import numpy as np
from jax import lax
from jax.experimental import pallas as pl
from jax.experimental.pallas import tpu as pltpu
from jax.sharding import PartitionSpec as P


GRID_W = 64
ROPE_BASE = 10000.0
NORM_EPS = 1e-06
LANES = 128
LIMIT = 12 << 20
KV_LIMIT = 56480000


VMEM = pl.BlockSpec(memory_space=pltpu.VMEM)
HBM = pl.BlockSpec(memory_space=pltpu.HBM)
NT = (((1,), (1,)), ((), ()))


def rope_tables(n_rows, head_dim):
    half = head_dim // 2
    quarter = half // 2
    inverse = ROPE_BASE ** (-np.arange(quarter, dtype=np.float64) * (2.0 / half))
    channel = np.arange(LANES) % head_dim
    freq = inverse[channel % quarter]
    sign = np.where(channel % half < quarter, -1.0, 1.0)
    by_row = channel < half

    def table(count, lanes):
        angles = np.arange(count, dtype=np.float64)[:, None] * freq[None, :]
        cosine = np.where(lanes[None, :], np.cos(angles), 0.0)
        sine = np.where(lanes[None, :], np.sin(angles) * sign[None, :], 0.0)
        return np.concatenate([cosine, sine], axis=1)

    pad = -n_rows % 8
    rows = np.concatenate([table(n_rows, by_row), np.zeros((pad, 2 * LANES))])
    return np.concatenate([table(GRID_W, ~by_row), rows]).astype(np.float32)


def turn(values, row_start, table_ref, head_dim):
    quarter = head_dim // 4
    rows = values.shape[0]
    lane = lax.broadcasted_iota(jnp.int32, (1, LANES), 1)
    ahead = pltpu.roll(values, LANES - quarter, 1)
    behind = pltpu.roll(values, quarter, 1)
    other = jnp.where(lane % (2 * quarter) < quarter, ahead, behind)
    columns = table_ref[0:GRID_W, :]
    out = []
    for j in range(rows // GRID_W):
        row = table_ref[pl.ds(GRID_W + row_start + j, 1), :]
        both = columns + row
        part = slice(j * GRID_W, (j + 1) * GRID_W)
        out.append(values[part] * both[:, :LANES] + other[part] * both[:, LANES:])
    return jnp.concatenate(out, axis=0)


def normed(values, gain, head_dim):
    lane = lax.broadcasted_iota(jnp.int32, (1, LANES), 1)
    gain = jnp.concatenate([gain] * (LANES // head_dim), axis=1)
    squares = values * values
    scale = jnp.zeros_like(values)
    for g in range(LANES // head_dim):
        mine = lane // head_dim == g
        mean = jnp.sum(jnp.where(mine, squares, 0.0), axis=1, keepdims=True) * (1.0 / head_dim)
        scale = jnp.where(mine, lax.rsqrt(mean + NORM_EPS), scale)
    return values * scale * gain


class Copies:
    def __init__(self, sems):
        self.sems = sems
        self.held = []

    def start(self, src, dst):
        copy = pltpu.make_async_copy(src, dst, self.sems.at[len(self.held)])
        copy.start()
        self.held.append(copy)

    def wait(self, first, last):
        for copy in self.held[first:last]:
            copy.wait()


def kv_kernel(
    head_dim, pieces, tok_hbm, wk_hbm, wv_hbm, gain_hbm, table_hbm,
    out_ref, tok_ref, both_ref, gain_ref, table_ref, sems,
):
    rows, width = tok_ref.shape
    step = width // pieces
    copies = Copies(sems)
    for i in range(pieces):
        part = pl.ds(i * step, step)
        copies.start(tok_hbm.at[:, part], tok_ref.at[:, part])
        copies.start(wk_hbm.at[:, part], both_ref.at[pl.ds(0, head_dim), part])
        copies.start(wv_hbm.at[:, part], both_ref.at[pl.ds(head_dim, head_dim), part])
    copies.start(gain_hbm, gain_ref)
    copies.start(table_hbm.at[:, pl.ds(0, 2 * LANES)], table_ref)
    raw = None
    for i in range(pieces):
        copies.wait(3 * i, 3 * i + 3)
        part = slice(i * step, (i + 1) * step)
        more = lax.dot_general(
            tok_ref[:, part], both_ref[:, part], NT, preferred_element_type=jnp.float32
        )
        raw = more if raw is None else raw + more
    raw = raw.astype(jnp.bfloat16).astype(jnp.float32)
    lane = lax.broadcasted_iota(jnp.int32, (1, LANES), 1)
    row_start = lax.axis_index("sp") * (rows // GRID_W)
    copies.wait(3 * pieces, 3 * pieces + 2)
    keys = turn(normed(raw, gain_ref[...], head_dim), row_start, table_ref, head_dim)
    out_ref[...] = jnp.where(lane < head_dim, keys, raw).astype(jnp.bfloat16)


def attend(qt, kv, head_dim, top, total, acc):
    scores = jnp.dot(kv, qt, preferred_element_type=jnp.float32)
    length, width = scores.shape
    new_top = jnp.max(scores, axis=0, keepdims=True)
    if top is not None:
        new_top = jnp.maximum(top, new_top)
    expos = jnp.exp(scores - new_top)
    part = jnp.sum(expos.reshape(length // 8, 8, width), axis=0)
    values = kv.astype(jnp.float32).T[head_dim : 2 * head_dim].astype(jnp.bfloat16)
    fresh = jnp.dot(values, expos.astype(jnp.bfloat16), preferred_element_type=jnp.float32)
    if top is None:
        return new_top, part, fresh
    shrink = jnp.exp(top - new_top)
    return new_top, total * shrink + part, acc * shrink + fresh


def attend_all(qt_ref, kv_refs, head_dim, state):
    for kv_ref in kv_refs:
        length = kv_ref.shape[0]
        step = length
        while step > 512:
            step //= 2
        if length == step:
            state = attend(qt_ref[...], kv_ref[...], head_dim, *state)
        else:

            def body(i, carry, kv_ref=kv_ref, step=step):
                at = pl.multiple_of(i * step, step)
                return attend(qt_ref[...], kv_ref[pl.ds(at, step), :], head_dim, *carry)

            state = lax.fori_loop(0, length // step, body, state)
    return state


def q_kernel(head_dim, tok_ref, wq_ref, gain_ref, table_ref, qt_ref):
    rows = tok_ref.shape[0]
    heads = wq_ref.shape[1] // head_dim
    raw = jnp.dot(tok_ref[...], wq_ref[...], preferred_element_type=jnp.float32)
    raw = raw.astype(jnp.bfloat16).astype(jnp.float32)
    row_start = lax.axis_index("sp") * (rows // GRID_W)
    per = LANES // head_dim
    columns = []
    for p in range(heads // per):
        x = raw[:, p * LANES : (p + 1) * LANES]
        y = turn(normed(x, gain_ref[...], head_dim), row_start, table_ref, head_dim)
        yt = (y * (head_dim ** -0.5)).T
        columns += [yt[g * head_dim : (g + 1) * head_dim] for g in range(per)]
    qt = jnp.concatenate(columns, axis=1)
    qt = jnp.concatenate([qt, jnp.zeros((LANES - head_dim, qt.shape[1]), jnp.float32)], axis=0)
    qt_ref[...] = qt.astype(jnp.bfloat16)


def first_kernel(head_dim, qt_ref, *refs):
    kv_refs = refs[:-3]
    top_ref, total_ref, acc_ref = refs[-3:]
    state = attend_all(qt_ref, kv_refs, head_dim, (None, None, None))
    top_ref[...], total_ref[...], acc_ref[...] = state


def block_kernel(head_dim, qt_ref, *refs):
    kv_refs = refs[:-6]
    top_in, total_in, acc_in, top_ref, total_ref, acc_ref = refs[-6:]
    state = attend_all(qt_ref, kv_refs, head_dim, (top_in[...], total_in[...], acc_in[...]))
    top_ref[...], total_ref[...], acc_ref[...] = state


def finish_kernel(head_dim, qt_ref, *refs):
    kv_refs = refs[:-5]
    top_in, total_in, acc_in, att_ref, log_ref = refs[-5:]
    state = attend_all(qt_ref, kv_refs, head_dim, (top_in[...], total_in[...], acc_in[...]))
    top, total, acc = state
    summed = jnp.sum(total, axis=0, keepdims=True)
    log = top + jnp.log(summed)
    out = acc / summed
    rows = att_ref.shape[0]
    heads = log_ref.shape[0]
    per = LANES // head_dim
    for h in range(heads):
        log_ref[h : h + 1, :] = log[:, h * rows : (h + 1) * rows]
    for p in range(heads // per):
        pair = [out[:, h * rows : (h + 1) * rows] for h in range(p * per, (p + 1) * per)]
        att = jnp.concatenate(pair, axis=0).T
        att_ref[:, p * LANES : (p + 1) * LANES] = att.astype(jnp.bfloat16)


def call(kernel, out_shape, flops, in_specs, limit=LIMIT, **more):
    return pl.pallas_call(
        kernel,
        out_shape=out_shape,
        in_specs=in_specs,
        out_specs=jax.tree.map(lambda _: VMEM, out_shape),
        cost_estimate=pl.CostEstimate(flops=flops, bytes_accessed=flops // 256, transcendentals=0),
        compiler_params=pltpu.CompilerParams(vmem_limit_bytes=limit),
        **more,
    )


def xor(n, bit):
    return [(i, i ^ bit) for i in range(n)]


def shards(n_sp, n_tp, tokens, w_query, w_key, w_value, w_output, query_gain, key_gain):
    head_dim = query_gain.shape[0]
    rows, width = tokens.shape
    heads = w_query.shape[1] // head_dim
    table = rope_tables(n_sp * rows // GRID_W, head_dim)
    wide = jnp.asarray(np.pad(table, ((0, 0), (0, 7 * table.shape[1]))))
    table = jnp.asarray(table)
    f32 = functools.partial(jax.ShapeDtypeStruct, dtype=jnp.float32)
    bf16 = functools.partial(jax.ShapeDtypeStruct, dtype=jnp.bfloat16)
    pieces = 4

    scratch = [pltpu.VMEM((1, head_dim), jnp.float32), pltpu.VMEM((table.shape[0], 2 * LANES), jnp.float32)]
    kv = call(
        functools.partial(kv_kernel, head_dim, pieces),
        bf16((rows, LANES)),
        2 * rows * width * LANES,
        [HBM] * 5,
        KV_LIMIT,
        scratch_shapes=[
            pltpu.VMEM(tokens.shape, jnp.bfloat16),
            pltpu.VMEM((LANES, width), jnp.bfloat16),
            *scratch,
            pltpu.SemaphoreType.DMA((3 * pieces + 2,)),
        ],
    )(tokens, w_key.T, w_value.T, key_gain[None, :], wide)

    size = heads * rows
    state_shape = [f32((1, size)), f32((8, size)), f32((head_dim, size))]

    def work(kvs):
        return sum(4 * size * x.shape[0] * LANES for x in kvs)

    qt = call(
        functools.partial(q_kernel, head_dim),
        bf16((LANES, size)),
        2 * rows * width * heads * head_dim,
        [VMEM] * 4,
    )(tokens, w_query, query_gain[None, :], table)

    def first(qt, *kvs):
        return call(
            functools.partial(first_kernel, head_dim),
            state_shape,
            work(kvs),
            [VMEM] * (1 + len(kvs)),
        )(qt, *kvs)

    def blocks(qt, state, *kvs):
        return call(
            functools.partial(block_kernel, head_dim),
            state_shape,
            work(kvs),
            [VMEM] * (4 + len(kvs)),
            input_output_aliases={1 + len(kvs) + i: i for i in range(3)},
        )(qt, *kvs, *state)

    def finish(qt, state, *kvs):
        return call(
            functools.partial(finish_kernel, head_dim),
            [bf16((rows, heads * head_dim)), f32((heads, rows))],
            work(kvs),
            [VMEM] * (4 + len(kvs)),
        )(qt, *kvs, *state)

    send = functools.partial(lax.ppermute, axis_name="sp")
    if n_sp == 8:
        near = send(kv, perm=xor(n_sp, 1))
        far = send(kv, perm=xor(n_sp, 6))
        pair = jnp.concatenate([kv, near], axis=0)
        middle = send(pair, perm=xor(n_sp, 4))
        beside = send(pair, perm=xor(n_sp, 2))
        far, qt = lax.optimization_barrier((far, qt))
        relayed = send(far, perm=xor(n_sp, 1))
        state = first(qt, pair)
        state = blocks(qt, state, beside)
        attended, log_sums = finish(qt, state, far, middle, relayed)
    else:
        held = kv
        state = None
        stride = 1
        pending = [kv]
        while stride < n_sp:
            radix = 2 if stride == 1 else min(4, n_sp // stride)
            got = [send(held, perm=xor(n_sp, d * stride)) for d in range(1, radix)]
            if state is None:
                state = first(qt, *pending)
            else:
                state = blocks(qt, state, *pending)
            pending = got
            stride *= radix
            if stride < n_sp:
                held = jnp.concatenate([held] + got, axis=0)
        attended, log_sums = finish(qt, state, *pending)

    own = rows // n_tp
    me = lax.axis_index("tp")

    def partial_out(block):
        part = lax.dynamic_slice_in_dim(attended, block * own, own, 0)
        return jnp.dot(part, w_output, preferred_element_type=jnp.float32)

    parts = {d: partial_out(me ^ d) for d in range(n_tp)}
    b = 1
    while b < n_tp:
        left = [d for d in parts if not d & b]
        sent = jnp.concatenate([parts[d ^ b].astype(jnp.bfloat16) for d in left], axis=0)
        got = lax.ppermute(sent, "tp", xor(n_tp, b)).astype(jnp.float32)
        parts = {d: parts[d] + got[i * own : (i + 1) * own] for i, d in enumerate(left)}
        b *= 2
    return parts[0].astype(jnp.bfloat16), log_sums


def solution(mesh):
    placed = (P("sp", None), P(None, "tp"), P(None, "tp"), P(None, "tp"), P("tp", None), P(), P())
    return jax.shard_map(
        functools.partial(shards, mesh.shape["sp"], mesh.shape["tp"]),
        mesh=mesh,
        in_specs=placed,
        out_specs=(P(("sp", "tp"), None), P("tp", "sp")),
        check_vma=False,
    )
```

profile of v0, /device:TPU:0, one launch (start us, length us, event | category | flops | bytes accessed | tf_op | source)
XLA Modules:
  0.0 34.8 jit_solution(10803207683771308413)
XLA Ops:
  0.6 0.0 copy-start
  0.6 0.0 copy-start.4
  0.7 0.7 %copy-done.4 = f32[64]{0:T(128)S(1)} copy-done((f32[64]{0:T(128)S(1)}, f32[64]{0:T(128)}, u32[]{:S(2)}) %copy-start.4) | copy-done | bytes 280
  1.4 0.0 copy-start.1
  1.4 0.0 copy-start.2
  1.4 2.4 %shard_map.104 = bf16[192,128]{1,0:T(8,128)(2,1)S(1)} custom-call(bf16[192,2048]{1,0:T(8,128)(2,1)} %tok_ref.1, bf16[64,2048]{1,0:T(8,128)(2,1)} %bitcast.10, bf16[64,2048]{1,0:T(8,128)(2,1)} %bitcast.11, f32[1,64]{1,0:T(1,128)S(1)} %bitcast.8, f32[88,2048]{1,0:T(8,128)} %constant.20.clone.table_hbm), custom_call_target="tpu_custom_call" | custom-call | flops 100663296 | bytes 393216 | tf_op jit(solution)/shard_map/pallas_call | solution.py:232
  3.8 0.0 copy-start.3
  3.8 3.1 %collective-permute-start.1 = (bf16[192,128]{1,0:T(8,128)(2,1)S(1)}, bf16[192,128]{1,0:T(8,128)(2,1)S(1)}, u32[]{:S(2)}, u32[]{:S(2)}) collective-permute-start(bf16[192,128]{1,0:T(8,128)(2,1)S(1)} %shard_map.104), channel_id=1, source_target_pairs={{0,4},{4,0},{8,12},{12,8},{16,20},{20,16},{24,28},{28,24},{1,5},{5... | collective-permute-start | bytes 147464 | tf_op jit(solution)/shard_map/ppermute | solution.py:286
  6.8 2.1 %collective-permute-done.1 = bf16[192,128]{1,0:T(8,128)(2,1)S(1)} collective-permute-done((bf16[192,128]{1,0:T(8,128)(2,1)S(1)}, bf16[192,128]{1,0:T(8,128)(2,1)S(1)}, u32[]{:S(2)}, u32[]{:S(2)}) %collective-permute-start.1) | collective-permute-done | bytes 49184 | tf_op jit(solution)/shard_map/ppermute | solution.py:286
  8.9 0.0 copy-start.5
  8.9 2.1 %collective-permute-start.4 = (bf16[384,128]{1,0:T(8,128)(2,1)S(1)}, bf16[384,128]{1,0:T(8,128)(2,1)S(1)}, u32[]{:S(2)}, u32[]{:S(2)}) collective-permute-start(bf16[384,128]{1,0:T(8,128)(2,1)S(1)} %pad_maximum_fusion.1.refs_0_), channel_id=1, source_target_pairs={{0,8},{4,12},{8,0},{12,4},{16,24},{20,28},{24,16},{28,20},{1,9},{5... | collective-permute-start | bytes 294920 | tf_op jit(solution)/shard_map/ppermute | solution.py:290
  11.1 2.5 %collective-permute-start = (bf16[192,128]{1,0:T(8,128)(2,1)S(1)}, bf16[192,128]{1,0:T(8,128)(2,1)S(1)}, u32[]{:S(2)}, u32[]{:S(2)}) collective-permute-start(bf16[192,128]{1,0:T(8,128)(2,1)S(1)} %shard_map.104), channel_id=1, source_target_pairs={{0,24},{4,28},{8,16},{12,20},{16,8},{20,12},{24,0},{28,4},{1,25},{... | collective-permute-start | bytes 147464 | tf_op jit(solution)/shard_map/ppermute | solution.py:287
  13.6 0.1 collective-permute-start.2
  13.7 0.0 copy-done.1
  13.7 0.0 copy-done.2
  13.7 0.0 copy-done.3
  13.7 0.0 copy-done.5
  13.7 0.8 %shard_map.105.qt_ref = bf16[128,768]{1,0:T(8,128)(2,1)S(1)} custom-call(bf16[192,2048]{1,0:T(8,128)(2,1)S(1)} %copy-done.1, bf16[2048,256]{1,0:T(8,128)(2,1)S(1)} %copy-done.2, f32[1,64]{1,0:T(1,128)S(1)} %bitcast.9, f32[88,256]{1,0:T(8,128)S(1)} %copy-done.3), custom_call_target="tpu_custom_call" | custom-call | flops 201326592 | bytes 786432 | tf_op jit(solution)/shard_map/pallas_call | solution.py:252
  14.5 3.3 %collective-permute-done.refs_0_ = bf16[192,128]{1,0:T(8,128)(2,1)S(1)} collective-permute-done((bf16[192,128]{1,0:T(8,128)(2,1)S(1)}, bf16[192,128]{1,0:T(8,128)(2,1)S(1)}, u32[]{:S(2)}, u32[]{:S(2)}) %collective-permute-start) | collective-permute-done | bytes 49184 | tf_op jit(solution)/shard_map/ppermute | solution.py:287
  17.8 1.5 %collective-permute-start.3 = (bf16[192,128]{1,0:T(8,128)(2,1)S(1)}, bf16[192,128]{1,0:T(8,128)(2,1)S(1)}, u32[]{:S(2)}, u32[]{:S(2)}) collective-permute-start(bf16[192,128]{1,0:T(8,128)(2,1)S(1)} %collective-permute-done.refs_0_), channel_id=1, source_target_pairs={{0,4},{4,0},{8,12},{12,8},{16,20},{20,16},{24,28},{28,24},{1,5},{5... | collective-permute-start | bytes 147464 | tf_op jit(solution)/shard_map/ppermute | solution.py:292
  19.3 0.6 %shard_map.106 = (f32[1,768]{1,0:T(1,128)S(1)}, f32[8,768]{1,0:T(8,128)S(1)}, f32[64,768]{1,0:T(8,128)S(1)}) custom-call(bf16[128,768]{1,0:T(8,128)(2,1)S(1)} %shard_map.105.qt_ref, bf16[384,128]{1,0:T(8,128)(2,1)S(1)} %pad_maximum_fusion.1.refs_0_), custom_call_target="tpu_custom_call" | custom-call | flops 150994944 | bytes 589824 | tf_op jit(solution)/shard_map/pallas_call | solution.py:260
  20.0 0.0 collective-permute-done.4.refs_0_
  20.0 0.8 %shard_map.107 = (f32[1,768]{1,0:T(1,128)S(1)}, f32[8,768]{1,0:T(8,128)S(1)}, f32[64,768]{1,0:T(8,128)S(1)}) custom-call(bf16[128,768]{1,0:T(8,128)(2,1)S(1)} %shard_map.105.qt_ref, bf16[384,128]{1,0:T(8,128)(2,1)S(1)} %collective-permute-done.4.refs_0_, ...), custom_call_target="tpu_custom_call", output_to_operand_aliasing={{0}: (2, {}), {1}: (3, {}), {2}: (4, {})} | custom-call | flops 150994944 | bytes 589824 | tf_op jit(solution)/shard_map/pallas_call | solution.py:268
  20.8 1.1 %collective-permute-done.3.refs_2_ = bf16[192,128]{1,0:T(8,128)(2,1)S(1)} collective-permute-done((bf16[192,128]{1,0:T(8,128)(2,1)S(1)}, bf16[192,128]{1,0:T(8,128)(2,1)S(1)}, u32[]{:S(2)}, u32[]{:S(2)}) %collective-permute-start.3) | collective-permute-done | bytes 49184 | tf_op jit(solution)/shard_map/ppermute | solution.py:292
  21.9 0.0 collective-permute-done.2.refs_1_
  21.9 2.1 %shard_map.108 = (bf16[192,256]{1,0:T(8,128)(2,1)S(1)}, f32[4,192]{1,0:T(4,128)}) custom-call(bf16[128,768]{1,0:T(8,128)(2,1)S(1)} %shard_map.105.qt_ref, bf16[192,128]{1,0:T(8,128)(2,1)S(1)} %collective-permute-done.refs_0_, bf16[384,128]{1,0:T(8,128)(2,1)S(1)} %collective-permute-done.2.refs_1_, bf16[192,128]{1,0:T(8,128)(2,1)S(1)} %collective-permute-done.3.refs_2_, ...), custom_call_target="tpu_custom_call" | custom-call | flops 301989888 | bytes 1179648 | tf_op jit(solution)/shard_map/pallas_call | solution.py:277
  24.0 0.0 copy-done
  24.0 0.3 convolution_convert_fusion
  24.3 0.3 convolution_convert_fusion.1
  24.6 0.1 collective-permute-start.5
  24.7 1.7 %collective-permute-done.5 = bf16[96,2048]{1,0:T(8,128)(2,1)S(1)} collective-permute-done((bf16[96,2048]{1,0:T(8,128)(2,1)S(1)}, bf16[96,2048]{1,0:T(8,128)(2,1)S(1)}, u32[]{:S(2)}, u32[]{:S(2)}) %collective-permute-start.5) | collective-permute-done | bytes 393248 | tf_op jit(solution)/shard_map/ppermute | solution.py:326
  26.4 0.1 convert_element_type.20
  26.5 0.3 fusion.2
  26.8 1.6 %collective-permute-start.6 = (bf16[48,2048]{1,0:T(8,128)(2,1)S(1)}, bf16[48,2048]{1,0:T(8,128)(2,1)S(1)}, u32[]{:S(2)}, u32[]{:S(2)}) collective-permute-start(bf16[48,2048]{1,0:T(8,128)(2,1)S(1)} %fusion.2), channel_id=1, source_target_pairs={{0,2},{1,3},{2,0},{3,1},{4,6},{5,7},{6,4},{7,5},{8,10},{9,11},{10,... | collective-permute-start | bytes 589832 | tf_op jit(solution)/shard_map/ppermute | solution.py:326
  28.4 5.4 %collective-permute-done.6 = bf16[48,2048]{1,0:T(8,128)(2,1)S(1)} collective-permute-done((bf16[48,2048]{1,0:T(8,128)(2,1)S(1)}, bf16[48,2048]{1,0:T(8,128)(2,1)S(1)}, u32[]{:S(2)}, u32[]{:S(2)}) %collective-permute-start.6) | collective-permute-done | bytes 196640 | tf_op jit(solution)/shard_map/ppermute | solution.py:326
  33.8 1.0 %fusion.1 = bf16[48,2048]{1,0:T(8,128)(2,1)} fusion(bf16[256,2048]{1,0:T(8,128)(2,1)S(1)} %copy-done, f32[96,2048]{1,0:T(8,128)S(1)} %convert_element_type.20, bf16[48,2048]{1,0:T(8,128)(2,1)S(1)} %collective-permute-done.6, bf16[192,256]{1,0:T(8,128)(2,1)S(1)} %get-tuple-element.20, s32[]{:T(128)S(6)} %select_n.12), kind=kOutput, calls=%fused_computation.3 | convolution fusion | flops 50724864 | bytes 1859588 | tf_op jit(solution)/shard_map/dot_general | solution.py:319
  (2 shorter events, 0.0 us)
Async XLA Ops:
  0.6 23.4 %copy-start = (bf16[256,2048]{1,0:T(8,128)(2,1)S(1)}, bf16[256,2048]{1,0:T(8,128)(2,1)}, u32[]{:S(2)}) copy-start(bf16[256,2048]{1,0:T(8,128)(2,1)} %param.13) | copy-start | bytes 3145732
  0.6 0.7 %copy-start.4 = (f32[64]{0:T(128)S(1)}, f32[64]{0:T(128)}, u32[]{:S(2)}) copy-start(f32[64]{0:T(128)} %param.15) | copy-start | bytes 772
  1.4 12.3 %copy-start.1 = (bf16[192,2048]{1,0:T(8,128)(2,1)S(1)}, bf16[192,2048]{1,0:T(8,128)(2,1)}, u32[]{:S(2)}) copy-start(bf16[192,2048]{1,0:T(8,128)(2,1)} %tok_ref.1) | copy-start | bytes 2359300
  1.4 12.3 %copy-start.2 = (bf16[2048,256]{1,0:T(8,128)(2,1)S(1)}, bf16[2048,256]{1,0:T(8,128)(2,1)}, u32[]{:S(2)}) copy-start(bf16[2048,256]{1,0:T(8,128)(2,1)} %wq_ref.1) | copy-start | bytes 3145732
  3.8 9.9 %copy-start.3 = (f32[88,256]{1,0:T(8,128)S(1)}, f32[88,256]{1,0:T(8,128)}, u32[]{:S(2)}) copy-start(f32[88,256]{1,0:T(8,128)} %constant.21.clone.table_ref) | copy-start | bytes 270340
  3.8 5.1 %collective-permute-start.1 = (bf16[192,128]{1,0:T(8,128)(2,1)S(1)}, bf16[192,128]{1,0:T(8,128)(2,1)S(1)}, u32[]{:S(2)}, u32[]{:S(2)}) collective-permute-start(bf16[192,128]{1,0:T(8,128)(2,1)S(1)} %shard_map.104), channel_id=1, source_target_pairs={{0,4},{4,0},{8,12},{12,8},{16,20},{20,16},{24,28},{28,24},{1,5},{5... | collective-permute-start | bytes 147464 | tf_op jit(solution)/shard_map/ppermute | solution.py:286
  8.9 4.8 %copy-start.5 = (f32[64]{0:T(128)S(1)}, f32[64]{0:T(128)}, u32[]{:S(2)}) copy-start(f32[64]{0:T(128)} %param.14) | copy-start | bytes 772
  8.9 11.1 %collective-permute-start.4 = (bf16[384,128]{1,0:T(8,128)(2,1)S(1)}, bf16[384,128]{1,0:T(8,128)(2,1)S(1)}, u32[]{:S(2)}, u32[]{:S(2)}) collective-permute-start(bf16[384,128]{1,0:T(8,128)(2,1)S(1)} %pad_maximum_fusion.1.refs_0_), channel_id=1, source_target_pairs={{0,8},{4,12},{8,0},{12,4},{16,24},{20,28},{24,16},{28,20},{1,9},{5... | collective-permute-start | bytes 294920 | tf_op jit(solution)/shard_map/ppermute | solution.py:290
  11.1 6.7 %collective-permute-start = (bf16[192,128]{1,0:T(8,128)(2,1)S(1)}, bf16[192,128]{1,0:T(8,128)(2,1)S(1)}, u32[]{:S(2)}, u32[]{:S(2)}) collective-permute-start(bf16[192,128]{1,0:T(8,128)(2,1)S(1)} %shard_map.104), channel_id=1, source_target_pairs={{0,24},{4,28},{8,16},{12,20},{16,8},{20,12},{24,0},{28,4},{1,25},{... | collective-permute-start | bytes 147464 | tf_op jit(solution)/shard_map/ppermute | solution.py:287
  13.6 8.4 %collective-permute-start.2 = (bf16[384,128]{1,0:T(8,128)(2,1)S(1)}, bf16[384,128]{1,0:T(8,128)(2,1)S(1)}, u32[]{:S(2)}, u32[]{:S(2)}) collective-permute-start(bf16[384,128]{1,0:T(8,128)(2,1)S(1)} %pad_maximum_fusion.1.refs_0_), channel_id=1, source_target_pairs={{0,16},{4,20},{8,24},{12,28},{16,0},{20,4},{24,8},{28,12},{1,17},{... | collective-permute-start | bytes 294920 | tf_op jit(solution)/shard_map/ppermute | solution.py:289
  17.8 4.1 %collective-permute-start.3 = (bf16[192,128]{1,0:T(8,128)(2,1)S(1)}, bf16[192,128]{1,0:T(8,128)(2,1)S(1)}, u32[]{:S(2)}, u32[]{:S(2)}) collective-permute-start(bf16[192,128]{1,0:T(8,128)(2,1)S(1)} %collective-permute-done.refs_0_), channel_id=1, source_target_pairs={{0,4},{4,0},{8,12},{12,8},{16,20},{20,16},{24,28},{28,24},{1,5},{5... | collective-permute-start | bytes 147464 | tf_op jit(solution)/shard_map/ppermute | solution.py:292
  24.6 1.8 %collective-permute-start.5 = (bf16[96,2048]{1,0:T(8,128)(2,1)S(1)}, bf16[96,2048]{1,0:T(8,128)(2,1)S(1)}, u32[]{:S(2)}, u32[]{:S(2)}) collective-permute-start(bf16[96,2048]{1,0:T(8,128)(2,1)S(1)} %pad_maximum_fusion), channel_id=1, source_target_pairs={{0,1},{1,0},{2,3},{3,2},{4,5},{5,4},{6,7},{7,6},{8,9},{9,8},{10,11... | collective-permute-start | bytes 1179656 | tf_op jit(solution)/shard_map/ppermute | solution.py:326
  26.8 7.0 %collective-permute-start.6 = (bf16[48,2048]{1,0:T(8,128)(2,1)S(1)}, bf16[48,2048]{1,0:T(8,128)(2,1)S(1)}, u32[]{:S(2)}, u32[]{:S(2)}) collective-permute-start(bf16[48,2048]{1,0:T(8,128)(2,1)S(1)} %fusion.2), channel_id=1, source_target_pairs={{0,2},{1,3},{2,0},{3,1},{4,6},{5,7},{6,4},{7,5},{8,10},{9,11},{10,... | collective-permute-start | bytes 589832 | tf_op jit(solution)/shard_map/ppermute | solution.py:326
where the time goes:
time: 34.9 us; the launch traced here: 34.8 us
  waiting for transfers between devices  13.7 us (39%)
  starting transfers between devices  11 us (32%)
  Pallas kernels  6.65 us (19%)
  matrix products  1.87 us (5%)
  local copies, waits for them, and re-layouts  0.77 us (2%)
  between operations  0.77 us (2%)
    ppermute x2, waiting for transfers between devices, shards(): got = lax.ppermute(sent, 'tp', xor(n_tp, b)).astype(jnp.float32)  7.15 us
    ppermute x1, waiting for transfers between devices, shards(): far = send(kv, perm=xor(n_sp, 6))  3.32 us
    ppermute x1, starting transfers between devices, shards(): near = send(kv, perm=xor(n_sp, 1))  3.06 us
    ppermute x1, starting transfers between devices, shards(): far = send(kv, perm=xor(n_sp, 6))  2.48 us
    pallas_call x1, Pallas kernels, shards(): call(functools.partial(kv_kernel, head_dim, pieces), bf16((rows, LANES)),...  2.37 us
    ppermute x1, starting transfers between devices, shards(): beside = send(pair, perm=xor(n_sp, 2))  2.14 us
    ppermute x1, waiting for transfers between devices, shards(): near = send(kv, perm=xor(n_sp, 1))  2.07 us
    pallas_call x1, Pallas kernels, finish(): call(functools.partial(finish_kernel, head_dim), [bf16((rows, heads * hea...  2.06 us
  transfers between devices with their start and end apart: 7, of which 5 were waited for; matrix products, arithmetic and copies ran while one was open for 0% of the time, Pallas kernels for 6%

commit v1 on v0

--- a/solution.py
+++ b/solution.py
@@ -183,22 +183,35 @@
 
 
 def finish_kernel(head_dim, qt_ref, *refs):
-    kv_refs = refs[:-5]
-    top_in, total_in, acc_in, att_ref, log_ref = refs[-5:]
+    kv_refs = refs[:-8]
+    top_in, total_in, acc_in, wo_ref, att_ref, top_ref, sum_ref, sent_ref = refs[-8:]
     state = attend_all(qt_ref, kv_refs, head_dim, (top_in[...], total_in[...], acc_in[...]))
     top, total, acc = state
     summed = jnp.sum(total, axis=0, keepdims=True)
-    log = top + jnp.log(summed)
-    out = acc / summed
+    out = acc * (1.0 / summed)
     rows = att_ref.shape[0]
-    heads = log_ref.shape[0]
+    heads = top_ref.shape[0]
     per = LANES // head_dim
-    for h in range(heads):
-        log_ref[h : h + 1, :] = log[:, h * rows : (h + 1) * rows]
     for p in range(heads // per):
         pair = [out[:, h * rows : (h + 1) * rows] for h in range(p * per, (p + 1) * per)]
         att = jnp.concatenate(pair, axis=0).T
         att_ref[:, p * LANES : (p + 1) * LANES] = att.astype(jnp.bfloat16)
+    own = sent_ref.shape[0]
+    sent_ref[...] = product(att_ref, wo_ref, rows // own - 1, own).astype(jnp.bfloat16)
+    for h in range(heads):
+        top_ref[h : h + 1, :] = top[:, h * rows : (h + 1) * rows]
+        sum_ref[h : h + 1, :] = summed[:, h * rows : (h + 1) * rows]
+
+
+def product(att_ref, wo_ref, d, own):
+    at = pl.multiple_of((lax.axis_index("tp") ^ d) * own, own)
+    return jnp.dot(att_ref[pl.ds(at, own), :], wo_ref[...], preferred_element_type=jnp.float32)
+
+
+def rest_kernel(att_ref, wo_ref, *out_refs):
+    for d, out_ref in enumerate(out_refs):
+        out = product(att_ref, wo_ref, d, out_ref.shape[0])
+        out_ref[...] = out.astype(out_ref.dtype)
 
 
 def call(kernel, out_shape, flops, in_specs, limit=LIMIT, **more):
@@ -226,7 +239,7 @@
     table = jnp.asarray(table)
     f32 = functools.partial(jax.ShapeDtypeStruct, dtype=jnp.float32)
     bf16 = functools.partial(jax.ShapeDtypeStruct, dtype=jnp.bfloat16)
-    pieces = 4
+    pieces = 1
 
     scratch = [pltpu.VMEM((1, head_dim), jnp.float32), pltpu.VMEM((table.shape[0], 2 * LANES), jnp.float32)]
     kv = call(
@@ -243,6 +256,7 @@
         ],
     )(tokens, w_key.T, w_value.T, key_gain[None, :], wide)
 
+    kv, tokens, w_query, w_output = lax.optimization_barrier((kv, tokens, w_query, w_output))
     size = heads * rows
     state_shape = [f32((1, size)), f32((8, size)), f32((head_dim, size))]
 
@@ -273,13 +287,20 @@
             input_output_aliases={1 + len(kvs) + i: i for i in range(3)},
         )(qt, *kvs, *state)
 
+    own = rows // n_tp
+
     def finish(qt, state, *kvs):
         return call(
             functools.partial(finish_kernel, head_dim),
-            [bf16((rows, heads * head_dim)), f32((heads, rows))],
+            [
+                bf16((rows, heads * head_dim)),
+                f32((heads, rows)),
+                f32((heads, rows)),
+                bf16((own, w_output.shape[1])),
+            ],
             work(kvs),
-            [VMEM] * (4 + len(kvs)),
-        )(qt, *kvs, *state)
+            [VMEM] * (5 + len(kvs)),
+        )(qt, *kvs, *state, w_output)
 
     send = functools.partial(lax.ppermute, axis_name="sp")
     if n_sp == 8:
@@ -288,11 +309,11 @@
         pair = jnp.concatenate([kv, near], axis=0)
         middle = send(pair, perm=xor(n_sp, 4))
         beside = send(pair, perm=xor(n_sp, 2))
-        far, qt = lax.optimization_barrier((far, qt))
         relayed = send(far, perm=xor(n_sp, 1))
         state = first(qt, pair)
-        state = blocks(qt, state, beside)
-        attended, log_sums = finish(qt, state, far, middle, relayed)
+        state = blocks(qt, state, beside, far)
+        state = blocks(qt, state, relayed)
+        attended, top, summed, sent = finish(qt, state, middle)
     else:
         held = kv
         state = None
@@ -309,24 +330,22 @@
             stride *= radix
             if stride < n_sp:
                 held = jnp.concatenate([held] + got, axis=0)
-        attended, log_sums = finish(qt, state, *pending)
-
-    own = rows // n_tp
-    me = lax.axis_index("tp")
-
-    def partial_out(block):
-        part = lax.dynamic_slice_in_dim(attended, block * own, own, 0)
-        return jnp.dot(part, w_output, preferred_element_type=jnp.float32)
-
-    parts = {d: partial_out(me ^ d) for d in range(n_tp)}
-    b = 1
-    while b < n_tp:
-        left = [d for d in parts if not d & b]
-        sent = jnp.concatenate([parts[d ^ b].astype(jnp.bfloat16) for d in left], axis=0)
-        got = lax.ppermute(sent, "tp", xor(n_tp, b)).astype(jnp.float32)
-        parts = {d: parts[d] + got[i * own : (i + 1) * own] for i, d in enumerate(left)}
-        b *= 2
-    return parts[0].astype(jnp.bfloat16), log_sums
+        attended, top, summed, sent = finish(qt, state, *pending)
+
+    parts = call(
+        rest_kernel,
+        [(bf16 if d % 2 else f32)(sent.shape) for d in range(n_tp - 1)],
+        2 * rows * w_output.size // n_tp,
+        [VMEM] * 2,
+    )(attended, w_output)
+    parts = [*parts, sent]
+    bit = 1
+    while bit < n_tp:
+        for d in reversed(range(0, n_tp, 2 * bit)):
+            got = lax.ppermute(parts[d + bit].astype(jnp.bfloat16), "tp", xor(n_tp, bit))
+            parts[d] = parts[d] + got.astype(jnp.float32)
+        bit *= 2
+    return parts[0].astype(jnp.bfloat16), top + jnp.log(summed)
 
 
 def solution(mesh):

time: 34.9 us -> 32.9 us (0.943)
  waiting for transfers between devices: 13.7 us -> 11.3 us
  matrix products: 1.87 us -> 0 us
  other arithmetic: 0.1 us -> 1.41 us
  starting transfers between devices: 11 us -> 11.5 us
  Pallas kernels: 6.65 us -> 7.07 us
    ppermute x2 -> x3, waiting for transfers between devices: 7.15 us -> 5.09 us  [shards(): lax.ppermute(parts[d + bit].astype(jnp.bfloat16), 'tp', xor(n_tp, bit))]
    dot_general x4 -> x0, matrix products: 1.87 us -> none  [partial_out(): return jnp.dot(part, w_output, preferred_element_type=jnp.float32)]
    ppermute x1, waiting for transfers between devices: 1.14 us -> 0.01 us  [shards(): relayed = send(far, perm=xor(n_sp, 1))]
    pallas_call x1 -> x2, Pallas kernels: 0.78 us -> 1.68 us  [blocks(): call(functools.partial(block_kernel, head_dim), state_shape, work(kvs), [...]
    pallas_call x1, Pallas kernels: 2.06 us -> 1.22 us  [finish(): call(functools.partial(finish_kernel, head_dim), [bf16((rows, heads * hea...]
    ppermute x1, waiting for transfers between devices: 3.32 us -> 4.15 us  [shards(): far = send(kv, perm=xor(n_sp, 6))]
    convert_element_type x1 -> x2, other arithmetic: 0.06 us -> 0.8 us  [the longest x1 0.75 us: shards(): return (parts[0].astype(jnp.bfloat16), top + jnp.log(summed))]
    pallas_call x0 -> x1, Pallas kernels: none -> 0.66 us  [shards(): call(rest_kernel, [(bf16 if d % 2 else f32)(sent.shape) for d in range(n_...]
  transfers between devices with their start and end apart: 7 -> 8, of which waited for: 5 -> 4; matrix products, arithmetic and copies ran while one was open for 0% -> 2% of each run, Pallas kernels for 6% -> 12%
where the time goes in v1:
time: 32.9 us; the launch traced here: 32.7 us
  starting transfers between devices  11.5 us (35%)
  waiting for transfers between devices  11.3 us (34%)
  Pallas kernels  7.07 us (21%)
  other arithmetic  1.41 us (4%)
  between operations  0.75 us (2%)
  local copies, waits for them, and re-layouts  0.69 us (2%)
    ppermute x3, waiting for transfers between devices, shards(): lax.ppermute(parts[d + bit].astype(jnp.bfloat16), 'tp', xor(n_tp, bit))  5.09 us
    ppermute x1, waiting for transfers between devices, shards(): far = send(kv, perm=xor(n_sp, 6))  4.15 us
    ppermute x1, starting transfers between devices, shards(): near = send(kv, perm=xor(n_sp, 1))  3.06 us
    ppermute x1, starting transfers between devices, shards(): far = send(kv, perm=xor(n_sp, 6))  2.48 us
    ppermute x3, starting transfers between devices, shards(): lax.ppermute(parts[d + bit].astype(jnp.bfloat16), 'tp', xor(n_tp, bit))  2.16 us
    ppermute x1, starting transfers between devices, shards(): beside = send(pair, perm=xor(n_sp, 2))  2.14 us
    ppermute x1, waiting for transfers between devices, shards(): near = send(kv, perm=xor(n_sp, 1))  2.06 us
    pallas_call x1, Pallas kernels, shards(): call(functools.partial(kv_kernel, head_dim, pieces), bf16((rows, LANES)),...  2.06 us
  transfers between devices with their start and end apart: 8, of which 4 were waited for; matrix products, arithmetic and copies ran while one was open for 2% of the time, Pallas kernels for 12%

profile of v1, /device:TPU:0, one launch (start us, length us, event | category | flops | bytes accessed | tf_op | source)
XLA Modules:
  0.0 32.7 jit_solution(15869532175745135934)
XLA Ops:
  0.6 0.0 copy-start.4
  0.6 0.6 %copy-done.4 = f32[64]{0:T(128)S(1)} copy-done((f32[64]{0:T(128)S(1)}, f32[64]{0:T(128)}, u32[]{:S(2)}) %copy-start.4) | copy-done | bytes 280
  1.3 0.0 copy-start.1
  1.3 0.0 copy-start.2
  1.3 2.1 %shard_map.104 = bf16[192,128]{1,0:T(8,128)(2,1)S(1)} custom-call(bf16[192,2048]{1,0:T(8,128)(2,1)} %tok_ref, bf16[64,2048]{1,0:T(8,128)(2,1)} %bitcast.6, bf16[64,2048]{1,0:T(8,128)(2,1)} %bitcast.7, f32[1,64]{1,0:T(1,128)S(1)} %bitcast.4, f32[88,2048]{1,0:T(8,128)} %constant.4.clone.table_hbm), custom_call_target="tpu_custom_call" | custom-call | flops 100663296 | bytes 393216 | tf_op jit(solution)/shard_map/pallas_call | solution.py:245
  3.4 0.0 copy-start.3
  3.4 3.1 %collective-permute-start = (bf16[192,128]{1,0:T(8,128)(2,1)S(1)}, bf16[192,128]{1,0:T(8,128)(2,1)S(1)}, u32[]{:S(2)}, u32[]{:S(2)}) collective-permute-start(bf16[192,128]{1,0:T(8,128)(2,1)S(1)} %shard_map.104), channel_id=1, source_target_pairs={{0,4},{4,0},{8,12},{12,8},{16,20},{20,16},{24,28},{28,24},{1,5},{5... | collective-permute-start | bytes 147464 | tf_op jit(solution)/shard_map/ppermute | solution.py:307
  6.4 2.1 %collective-permute-done = bf16[192,128]{1,0:T(8,128)(2,1)S(1)} collective-permute-done((bf16[192,128]{1,0:T(8,128)(2,1)S(1)}, bf16[192,128]{1,0:T(8,128)(2,1)S(1)}, u32[]{:S(2)}, u32[]{:S(2)}) %collective-permute-start) | collective-permute-done | bytes 49184 | tf_op jit(solution)/shard_map/ppermute | solution.py:307
  8.5 0.0 copy-start.5
  8.5 2.1 %collective-permute-start.4 = (bf16[384,128]{1,0:T(8,128)(2,1)S(1)}, bf16[384,128]{1,0:T(8,128)(2,1)S(1)}, u32[]{:S(2)}, u32[]{:S(2)}) collective-permute-start(bf16[384,128]{1,0:T(8,128)(2,1)S(1)} %constant_dynamic-update-slice_fusion.refs_0_), channel_id=1, source_target_pairs={{0,8},{4,12},{8,0},{12,4},{16,24},{20,28},{24,16},{28,20},{1,9},{5... | collective-permute-start | bytes 294920 | tf_op jit(solution)/shard_map/ppermute | solution.py:311
  10.7 2.5 %collective-permute-start.2 = (bf16[192,128]{1,0:T(8,128)(2,1)S(1)}, bf16[192,128]{1,0:T(8,128)(2,1)S(1)}, u32[]{:S(2)}, u32[]{:S(2)}) collective-permute-start(bf16[192,128]{1,0:T(8,128)(2,1)S(1)} %shard_map.104), channel_id=1, source_target_pairs={{0,24},{4,28},{8,16},{12,20},{16,8},{20,12},{24,0},{28,4},{1,25},{... | collective-permute-start | bytes 147464 | tf_op jit(solution)/shard_map/ppermute | solution.py:308
  13.1 0.1 collective-permute-start.1
  13.3 4.2 %collective-permute-done.2.refs_1_ = bf16[192,128]{1,0:T(8,128)(2,1)S(1)} collective-permute-done((bf16[192,128]{1,0:T(8,128)(2,1)S(1)}, bf16[192,128]{1,0:T(8,128)(2,1)S(1)}, u32[]{:S(2)}, u32[]{:S(2)}) %collective-permute-start.2) | collective-permute-done | bytes 49184 | tf_op jit(solution)/shard_map/ppermute | solution.py:308
  17.4 1.5 %collective-permute-start.3 = (bf16[192,128]{1,0:T(8,128)(2,1)S(1)}, bf16[192,128]{1,0:T(8,128)(2,1)S(1)}, u32[]{:S(2)}, u32[]{:S(2)}) collective-permute-start(bf16[192,128]{1,0:T(8,128)(2,1)S(1)} %collective-permute-done.2.refs_1_), channel_id=1, source_target_pairs={{0,4},{4,0},{8,12},{12,8},{16,20},{20,16},{24,28},{28,24},{1,5},{5... | collective-permute-start | bytes 147464 | tf_op jit(solution)/shard_map/ppermute | solution.py:312
  18.9 0.0 copy-done.1
  18.9 0.0 copy-done.2
  18.9 0.0 copy-done.3
  18.9 0.0 copy-done.5
  19.0 0.8 %shard_map.105.qt_ref = bf16[128,768]{1,0:T(8,128)(2,1)S(1)} custom-call(bf16[192,2048]{1,0:T(8,128)(2,1)S(1)} %copy-done.1, bf16[2048,256]{1,0:T(8,128)(2,1)S(1)} %copy-done.2, f32[1,64]{1,0:T(1,128)S(1)} %bitcast.5, f32[88,256]{1,0:T(8,128)S(1)} %copy-done.3), custom_call_target="tpu_custom_call" | custom-call | flops 201326592 | bytes 786432 | tf_op jit(solution)/shard_map/pallas_call | solution.py:266
  19.8 0.0 copy-start
  19.8 0.6 %shard_map.106 = (f32[1,768]{1,0:T(1,128)S(1)}, f32[8,768]{1,0:T(8,128)S(1)}, f32[64,768]{1,0:T(8,128)S(1)}) custom-call(bf16[128,768]{1,0:T(8,128)(2,1)S(1)} %shard_map.105.qt_ref, bf16[384,128]{1,0:T(8,128)(2,1)S(1)} %constant_dynamic-update-slice_fusion.refs_0_), custom_call_target="tpu_custom_call" | custom-call | flops 150994944 | bytes 589824 | tf_op jit(solution)/shard_map/pallas_call | solution.py:274
  20.4 0.0 collective-permute-done.4.refs_0_
  20.4 1.2 %shard_map.107 = (f32[1,768]{1,0:T(1,128)S(1)}, f32[8,768]{1,0:T(8,128)S(1)}, f32[64,768]{1,0:T(8,128)S(1)}) custom-call(bf16[128,768]{1,0:T(8,128)(2,1)S(1)} %shard_map.105.qt_ref, bf16[384,128]{1,0:T(8,128)(2,1)S(1)} %collective-permute-done.4.refs_0_, ...), custom_call_target="tpu_custom_call", output_to_operand_aliasing={{0}: (3, {}), {1}: (4, {}), {2}: (5, {})} | custom-call | flops 226492416 | bytes 884736 | tf_op jit(solution)/shard_map/pallas_call | solution.py:282
  21.6 0.0 collective-permute-done.3.refs_0_
  21.6 0.5 %shard_map.108 = (f32[1,768]{1,0:T(1,128)S(1)}, f32[8,768]{1,0:T(8,128)S(1)}, f32[64,768]{1,0:T(8,128)S(1)}) custom-call(bf16[128,768]{1,0:T(8,128)(2,1)S(1)} %shard_map.105.qt_ref, bf16[192,128]{1,0:T(8,128)(2,1)S(1)} %collective-permute-done.3.refs_0_, ...), custom_call_target="tpu_custom_call", output_to_operand_aliasing={{0}: (2, {}), {1}: (3, {}), {2}: (4, {})} | custom-call | flops 75497472 | bytes 294912 | tf_op jit(solution)/shard_map/pallas_call | solution.py:282
  22.1 0.0 collective-permute-done.1.refs_0_
  22.1 0.0 copy-done
  22.2 1.2 %shard_map.109 = (bf16[192,256]{1,0:T(8,128)(2,1)S(1)}, f32[4,192]{1,0:T(4,128)S(1)}, f32[4,192]{1,0:T(4,128)S(1)}, bf16[48,2048]{1,0:T(8,128)(2,1)S(1)}) custom-call(bf16[128,768]{1,0:T(8,128)(2,1)S(1)} %shard_map.105.qt_ref, bf16[384,128]{1,0:T(8,128)(2,1)S(1)} %collective-permute-done.1.refs_0_, f32[1,768]{1,0:T(1,128)S(1)} %get-tuple-element.31.refs_1_, ...), custom_call_target="tpu_custom_call" | custom-call | flops 150994944 | bytes 589824 | tf_op jit(solution)/shard_map/pallas_call | solution.py:293
  23.4 0.1 collective-permute-start.6
  23.5 0.7 %shard_map.110 = (f32[48,2048]{1,0:T(8,128)S(1)}, bf16[48,2048]{1,0:T(8,128)(2,1)S(1)}, f32[48,2048]{1,0:T(8,128)S(1)}) custom-call(bf16[192,256]{1,0:T(8,128)(2,1)S(1)} %get-tuple-element.35.att_ref, bf16[256,2048]{1,0:T(8,128)(2,1)S(1)} %copy-done), custom_call_target="tpu_custom_call" | custom-call | flops 50331648 | bytes 196608 | tf_op jit(solution)/shard_map/pallas_call | solution.py:335
  24.1 0.5 %collective-permute-start.5 = (bf16[48,2048]{1,0:T(8,128)(2,1)S(1)}, bf16[48,2048]{1,0:T(8,128)(2,1)S(1)}, u32[]{:S(2)}, u32[]{:S(2)}) collective-permute-start(bf16[48,2048]{1,0:T(8,128)(2,1)S(1)} %get-tuple-element.37), channel_id=1, source_target_pairs={{0,1},{1,0},{2,3},{3,2},{4,5},{5,4},{6,7},{7,6},{8,9},{9,8},{10,11... | collective-permute-start | bytes 589832 | tf_op jit(solution)/shard_map/ppermute | solution.py:345
  24.7 0.2 collective-permute-done.6
  24.9 0.1 add_convert_fusion.1
  24.9 1.6 %collective-permute-start.7 = (bf16[48,2048]{1,0:T(8,128)(2,1)S(1)}, bf16[48,2048]{1,0:T(8,128)(2,1)S(1)}, u32[]{:S(2)}, u32[]{:S(2)}) collective-permute-start(bf16[48,2048]{1,0:T(8,128)(2,1)S(1)} %add_convert_fusion.1), channel_id=1, source_target_pairs={{0,2},{1,3},{2,0},{3,1},{4,6},{5,7},{6,4},{7,5},{8,10},{9,11},{10,... | collective-permute-start | bytes 589832 | tf_op jit(solution)/shard_map/ppermute | solution.py:345
  26.5 0.6 %log_add_fusion = f32[4,192]{1,0:T(4,128)} fusion(f32[4,192]{1,0:T(4,128)S(1)} %get-tuple-element.40, f32[4,192]{1,0:T(4,128)S(1)} %get-tuple-element.41), kind=kLoop, calls=%fused_computation.4 | loop fusion | flops 768 | bytes 9216 | tf_op jit(solution)/shard_map/add | solution.py:348
  27.1 0.0 collective-permute-done.5
  27.1 4.9 %collective-permute-done.7 = bf16[48,2048]{1,0:T(8,128)(2,1)S(1)} collective-permute-done((bf16[48,2048]{1,0:T(8,128)(2,1)S(1)}, bf16[48,2048]{1,0:T(8,128)(2,1)S(1)}, u32[]{:S(2)}, u32[]{:S(2)}) %collective-permute-start.7) | collective-permute-done | bytes 196640 | tf_op jit(solution)/shard_map/ppermute | solution.py:345
  31.9 0.8 %add_convert_fusion = bf16[48,2048]{1,0:T(8,128)(2,1)} fusion(bf16[48,2048]{1,0:T(8,128)(2,1)S(1)} %collective-permute-done.7, f32[48,2048]{1,0:T(8,128)S(1)} %get-tuple-element.36, bf16[48,2048]{1,0:T(8,128)(2,1)S(1)} %collective-permute-done.5), kind=kLoop, calls=%fused_computation | loop fusion | flops 491520 | bytes 983040 | tf_op jit(solution)/shard_map/convert_element_type | solution.py:348
  (2 shorter events, 0.0 us)
Async XLA Ops:
  0.6 0.7 %copy-start.4 = (f32[64]{0:T(128)S(1)}, f32[64]{0:T(128)}, u32[]{:S(2)}) copy-start(f32[64]{0:T(128)} %param.15) | copy-start | bytes 772
  1.3 17.7 %copy-start.1 = (bf16[192,2048]{1,0:T(8,128)(2,1)S(1)}, bf16[192,2048]{1,0:T(8,128)(2,1)}, u32[]{:S(2)}) copy-start(bf16[192,2048]{1,0:T(8,128)(2,1)} %tok_ref) | copy-start | bytes 2359300
  1.3 17.7 %copy-start.2 = (bf16[2048,256]{1,0:T(8,128)(2,1)S(1)}, bf16[2048,256]{1,0:T(8,128)(2,1)}, u32[]{:S(2)}) copy-start(bf16[2048,256]{1,0:T(8,128)(2,1)} %wq_ref) | copy-start | bytes 3145732
  3.4 15.6 %copy-start.3 = (f32[88,256]{1,0:T(8,128)S(1)}, f32[88,256]{1,0:T(8,128)}, u32[]{:S(2)}) copy-start(f32[88,256]{1,0:T(8,128)} %constant.5.clone.table_ref) | copy-start | bytes 270340
  3.4 5.1 %collective-permute-start = (bf16[192,128]{1,0:T(8,128)(2,1)S(1)}, bf16[192,128]{1,0:T(8,128)(2,1)S(1)}, u32[]{:S(2)}, u32[]{:S(2)}) collective-permute-start(bf16[192,128]{1,0:T(8,128)(2,1)S(1)} %shard_map.104), channel_id=1, source_target_pairs={{0,4},{4,0},{8,12},{12,8},{16,20},{20,16},{24,28},{28,24},{1,5},{5... | collective-permute-start | bytes 147464 | tf_op jit(solution)/shard_map/ppermute | solution.py:307
  8.5 10.4 %copy-start.5 = (f32[64]{0:T(128)S(1)}, f32[64]{0:T(128)}, u32[]{:S(2)}) copy-start(f32[64]{0:T(128)} %param.14) | copy-start | bytes 772
  8.5 11.9 %collective-permute-start.4 = (bf16[384,128]{1,0:T(8,128)(2,1)S(1)}, bf16[384,128]{1,0:T(8,128)(2,1)S(1)}, u32[]{:S(2)}, u32[]{:S(2)}) collective-permute-start(bf16[384,128]{1,0:T(8,128)(2,1)S(1)} %constant_dynamic-update-slice_fusion.refs_0_), channel_id=1, source_target_pairs={{0,8},{4,12},{8,0},{12,4},{16,24},{20,28},{24,16},{28,20},{1,9},{5... | collective-permute-start | bytes 294920 | tf_op jit(solution)/shard_map/ppermute | solution.py:311
  10.7 6.7 %collective-permute-start.2 = (bf16[192,128]{1,0:T(8,128)(2,1)S(1)}, bf16[192,128]{1,0:T(8,128)(2,1)S(1)}, u32[]{:S(2)}, u32[]{:S(2)}) collective-permute-start(bf16[192,128]{1,0:T(8,128)(2,1)S(1)} %shard_map.104), channel_id=1, source_target_pairs={{0,24},{4,28},{8,16},{12,20},{16,8},{20,12},{24,0},{28,4},{1,25},{... | collective-permute-start | bytes 147464 | tf_op jit(solution)/shard_map/ppermute | solution.py:308
  13.1 9.0 %collective-permute-start.1 = (bf16[384,128]{1,0:T(8,128)(2,1)S(1)}, bf16[384,128]{1,0:T(8,128)(2,1)S(1)}, u32[]{:S(2)}, u32[]{:S(2)}) collective-permute-start(bf16[384,128]{1,0:T(8,128)(2,1)S(1)} %constant_dynamic-update-slice_fusion.refs_0_), channel_id=1, source_target_pairs={{0,16},{4,20},{8,24},{12,28},{16,0},{20,4},{24,8},{28,12},{1,17},{... | collective-permute-start | bytes 294920 | tf_op jit(solution)/shard_map/ppermute | solution.py:310
  17.4 4.2 %collective-permute-start.3 = (bf16[192,128]{1,0:T(8,128)(2,1)S(1)}, bf16[192,128]{1,0:T(8,128)(2,1)S(1)}, u32[]{:S(2)}, u32[]{:S(2)}) collective-permute-start(bf16[192,128]{1,0:T(8,128)(2,1)S(1)} %collective-permute-done.2.refs_1_), channel_id=1, source_target_pairs={{0,4},{4,0},{8,12},{12,8},{16,20},{20,16},{24,28},{28,24},{1,5},{5... | collective-permute-start | bytes 147464 | tf_op jit(solution)/shard_map/ppermute | solution.py:312
  19.8 2.4 %copy-start = (bf16[256,2048]{1,0:T(8,128)(2,1)S(1)}, bf16[256,2048]{1,0:T(8,128)(2,1)}, u32[]{:S(2)}) copy-start(bf16[256,2048]{1,0:T(8,128)(2,1)} %wo_ref) | copy-start | bytes 3145732
  23.4 1.5 %collective-permute-start.6 = (bf16[48,2048]{1,0:T(8,128)(2,1)S(1)}, bf16[48,2048]{1,0:T(8,128)(2,1)S(1)}, u32[]{:S(2)}, u32[]{:S(2)}) collective-permute-start(bf16[48,2048]{1,0:T(8,128)(2,1)S(1)} %get-tuple-element.39), channel_id=1, source_target_pairs={{0,1},{1,0},{2,3},{3,2},{4,5},{5,4},{6,7},{7,6},{8,9},{9,8},{10,11... | collective-permute-start | bytes 589832 | tf_op jit(solution)/shard_map/ppermute | solution.py:345
  24.1 3.0 %collective-permute-start.5 = (bf16[48,2048]{1,0:T(8,128)(2,1)S(1)}, bf16[48,2048]{1,0:T(8,128)(2,1)S(1)}, u32[]{:S(2)}, u32[]{:S(2)}) collective-permute-start(bf16[48,2048]{1,0:T(8,128)(2,1)S(1)} %get-tuple-element.37), channel_id=1, source_target_pairs={{0,1},{1,0},{2,3},{3,2},{4,5},{5,4},{6,7},{7,6},{8,9},{9,8},{10,11... | collective-permute-start | bytes 589832 | tf_op jit(solution)/shard_map/ppermute | solution.py:345
  24.9 7.0 %collective-permute-start.7 = (bf16[48,2048]{1,0:T(8,128)(2,1)S(1)}, bf16[48,2048]{1,0:T(8,128)(2,1)S(1)}, u32[]{:S(2)}, u32[]{:S(2)}) collective-permute-start(bf16[48,2048]{1,0:T(8,128)(2,1)S(1)} %add_convert_fusion.1), channel_id=1, source_target_pairs={{0,2},{1,3},{2,0},{3,1},{4,6},{5,7},{6,4},{7,5},{8,10},{9,11},{10,... | collective-permute-start | bytes 589832 | tf_op jit(solution)/shard_map/ppermute | solution.py:345

commit v2 on v1

--- a/solution.py
+++ b/solution.py
@@ -14,6 +14,7 @@
 NORM_EPS = 1e-06
 LANES = 128
 LIMIT = 12 << 20
+SPAN = 768
 KV_LIMIT = 56480000
 
 
@@ -116,35 +117,52 @@
     out_ref[...] = jnp.where(lane < head_dim, keys, raw).astype(jnp.bfloat16)
 
 
-def attend(qt, kv, head_dim, top, total, acc):
-    scores = jnp.dot(kv, qt, preferred_element_type=jnp.float32)
-    length, width = scores.shape
-    new_top = jnp.max(scores, axis=0, keepdims=True)
+def attend(qt, kvs, head_dim, top, total, acc, score_ref, weight_ref):
+    width = qt.shape[1]
+    count = 0
+    eight = None
+    values = []
+    for kv in kvs:
+        scores = jnp.dot(kv, qt, preferred_element_type=jnp.float32)
+        score_ref[count : count + kv.shape[0], :] = scores
+        for i in range(0, kv.shape[0], 8):
+            most = score_ref[count + i : count + i + 8, :]
+            eight = most if eight is None else jnp.maximum(eight, most)
+        values.append(kv.astype(jnp.float32).T[head_dim : 2 * head_dim].astype(jnp.bfloat16))
+        count += kv.shape[0]
+    new_top = jnp.max(eight, axis=0, keepdims=True)
     if top is not None:
         new_top = jnp.maximum(top, new_top)
-    expos = jnp.exp(scores - new_top)
-    part = jnp.sum(expos.reshape(length // 8, 8, width), axis=0)
-    values = kv.astype(jnp.float32).T[head_dim : 2 * head_dim].astype(jnp.bfloat16)
-    fresh = jnp.dot(values, expos.astype(jnp.bfloat16), preferred_element_type=jnp.float32)
+    part = jnp.zeros((8, width), jnp.float32)
+    for at in range(0, count, 16):
+        expos = jnp.exp(score_ref[at : at + 16, :] - new_top)
+        weight_ref[at : at + 16, :] = expos.astype(jnp.bfloat16)
+        part = part + (expos[:8] + expos[8:])
+    values = jnp.concatenate(values, axis=1)
+    fresh = jnp.dot(values, weight_ref[0:count, :], preferred_element_type=jnp.float32)
     if top is None:
         return new_top, part, fresh
     shrink = jnp.exp(top - new_top)
     return new_top, total * shrink + part, acc * shrink + fresh
 
 
-def attend_all(qt_ref, kv_refs, head_dim, state):
+def attend_all(qt_ref, kv_refs, head_dim, state, score_ref, weight_ref):
+    spare = head_dim, *state, score_ref, weight_ref
+    if sum(kv_ref.shape[0] for kv_ref in kv_refs) <= SPAN:
+        return attend(qt_ref[...], [kv_ref[...] for kv_ref in kv_refs], *spare)
     for kv_ref in kv_refs:
         length = kv_ref.shape[0]
         step = length
-        while step > 512:
+        while step > SPAN:
             step //= 2
         if length == step:
-            state = attend(qt_ref[...], kv_ref[...], head_dim, *state)
+            state = attend(qt_ref[...], [kv_ref[...]], head_dim, *state, score_ref, weight_ref)
         else:
 
             def body(i, carry, kv_ref=kv_ref, step=step):
                 at = pl.multiple_of(i * step, step)
-                return attend(qt_ref[...], kv_ref[pl.ds(at, step), :], head_dim, *carry)
+                kvs = [kv_ref[pl.ds(at, step), :]]
+                return attend(qt_ref[...], kvs, head_dim, *carry, score_ref, weight_ref)
 
             state = lax.fori_loop(0, length // step, body, state)
     return state
@@ -169,23 +187,23 @@
 
 
 def first_kernel(head_dim, qt_ref, *refs):
-    kv_refs = refs[:-3]
-    top_ref, total_ref, acc_ref = refs[-3:]
-    state = attend_all(qt_ref, kv_refs, head_dim, (None, None, None))
+    kv_refs = refs[:-5]
+    top_ref, total_ref, acc_ref, *spare = refs[-5:]
+    state = attend_all(qt_ref, kv_refs, head_dim, (None, None, None), *spare)
     top_ref[...], total_ref[...], acc_ref[...] = state
 
 
 def block_kernel(head_dim, qt_ref, *refs):
-    kv_refs = refs[:-6]
-    top_in, total_in, acc_in, top_ref, total_ref, acc_ref = refs[-6:]
-    state = attend_all(qt_ref, kv_refs, head_dim, (top_in[...], total_in[...], acc_in[...]))
+    kv_refs = refs[:-8]
+    top_in, total_in, acc_in, top_ref, total_ref, acc_ref, *spare = refs[-8:]
+    state = attend_all(qt_ref, kv_refs, head_dim, (top_in[...], total_in[...], acc_in[...]), *spare)
     top_ref[...], total_ref[...], acc_ref[...] = state
 
 
 def finish_kernel(head_dim, qt_ref, *refs):
-    kv_refs = refs[:-8]
-    top_in, total_in, acc_in, wo_ref, att_ref, top_ref, sum_ref, sent_ref = refs[-8:]
-    state = attend_all(qt_ref, kv_refs, head_dim, (top_in[...], total_in[...], acc_in[...]))
+    kv_refs = refs[:-10]
+    top_in, total_in, acc_in, wo_ref, att_ref, top_ref, sum_ref, sent_ref, *spare = refs[-10:]
+    state = attend_all(qt_ref, kv_refs, head_dim, (top_in[...], total_in[...], acc_in[...]), *spare)
     top, total, acc = state
     summed = jnp.sum(total, axis=0, keepdims=True)
     out = acc * (1.0 / summed)
@@ -260,6 +278,10 @@
     size = heads * rows
     state_shape = [f32((1, size)), f32((8, size)), f32((head_dim, size))]
 
+    def spare(kvs):
+        count = min(SPAN, sum(x.shape[0] for x in kvs))
+        return [pltpu.VMEM((count, size), jnp.float32), pltpu.VMEM((count, size), jnp.bfloat16)]
+
     def work(kvs):
         return sum(4 * size * x.shape[0] * LANES for x in kvs)
 
@@ -276,6 +298,7 @@
             state_shape,
             work(kvs),
             [VMEM] * (1 + len(kvs)),
+            scratch_shapes=spare(kvs),
         )(qt, *kvs)
 
     def blocks(qt, state, *kvs):
@@ -284,6 +307,7 @@
             state_shape,
             work(kvs),
             [VMEM] * (4 + len(kvs)),
+            scratch_shapes=spare(kvs),
             input_output_aliases={1 + len(kvs) + i: i for i in range(3)},
         )(qt, *kvs, *state)
 
@@ -300,20 +324,20 @@
             ],
             work(kvs),
             [VMEM] * (5 + len(kvs)),
+            scratch_shapes=spare(kvs),
         )(qt, *kvs, *state, w_output)
 
     send = functools.partial(lax.ppermute, axis_name="sp")
     if n_sp == 8:
         near = send(kv, perm=xor(n_sp, 1))
-        far = send(kv, perm=xor(n_sp, 6))
+        far = send(kv, perm=xor(n_sp, 4))
         pair = jnp.concatenate([kv, near], axis=0)
-        middle = send(pair, perm=xor(n_sp, 4))
+        middle = send(pair, perm=xor(n_sp, 6))
         beside = send(pair, perm=xor(n_sp, 2))
         relayed = send(far, perm=xor(n_sp, 1))
         state = first(qt, pair)
         state = blocks(qt, state, beside, far)
-        state = blocks(qt, state, relayed)
-        attended, top, summed, sent = finish(qt, state, middle)
+        attended, top, summed, sent = finish(qt, state, relayed, middle)
     else:
         held = kv
         state = None

time: 32.9 us -> 30.6 us (0.930)
  waiting for transfers between devices: 11.3 us -> 9.61 us
  Pallas kernels: 7.07 us -> 6.59 us
    ppermute x2, waiting for transfers between devices: 4.16 us -> 2.4 us  [the longest x1 2.4 us: shards(): far = send(kv, perm=xor(n_sp, 4))]
    pallas_call x2 -> x1, Pallas kernels: 1.68 us -> 1.02 us  [blocks(): call(functools.partial(block_kernel, head_dim), state_shape, work(kvs), [...]
  transfers between devices with their start and end apart: 8 -> 8, of which waited for: 4 -> 5; matrix products, arithmetic and copies ran while one was open for 2% -> 2% of each run, Pallas kernels for 12% -> 10%
where the time goes in v2:
time: 30.6 us; the launch traced here: 30.5 us
  starting transfers between devices  11.5 us (38%)
  waiting for transfers between devices  9.61 us (31%)
  Pallas kernels  6.59 us (22%)
  other arithmetic  1.39 us (5%)
  between operations  0.73 us (2%)
  local copies, waits for them, and re-layouts  0.69 us (2%)
    ppermute x3, waiting for transfers between devices, shards(): lax.ppermute(parts[d + bit].astype(jnp.bfloat16), 'tp', xor(n_tp, bit))  5.09 us
    ppermute x1, starting transfers between devices, shards(): near = send(kv, perm=xor(n_sp, 1))  3.06 us
    ppermute x1, starting transfers between devices, shards(): far = send(kv, perm=xor(n_sp, 4))  2.59 us
    ppermute x1, waiting for transfers between devices, shards(): far = send(kv, perm=xor(n_sp, 4))  2.4 us
    ppermute x3, starting transfers between devices, shards(): lax.ppermute(parts[d + bit].astype(jnp.bfloat16), 'tp', xor(n_tp, bit))  2.16 us
    ppermute x1, starting transfers between devices, shards(): beside = send(pair, perm=xor(n_sp, 2))  2.14 us
    ppermute x1, waiting for transfers between devices, shards(): near = send(kv, perm=xor(n_sp, 1))  2.06 us
    pallas_call x1, Pallas kernels, shards(): call(functools.partial(kv_kernel, head_dim, pieces), bf16((rows, LANES)),...  2.06 us
  transfers between devices with their start and end apart: 8, of which 5 were waited for; matrix products, arithmetic and copies ran while one was open for 2% of the time, Pallas kernels for 10%

profile of v2, /device:TPU:0, one launch (start us, length us, event | category | flops | bytes accessed | tf_op | source)
XLA Modules:
  0.0 30.5 jit_solution(6415411224089534308)
XLA Ops:
  0.6 0.0 copy-start.4
  0.6 0.6 %copy-done.4 = f32[64]{0:T(128)S(1)} copy-done((f32[64]{0:T(128)S(1)}, f32[64]{0:T(128)}, u32[]{:S(2)}) %copy-start.4) | copy-done | bytes 280
  1.3 0.0 copy-start.1
  1.3 0.0 copy-start.2
  1.3 2.1 %shard_map.104 = bf16[192,128]{1,0:T(8,128)(2,1)S(1)} custom-call(bf16[192,2048]{1,0:T(8,128)(2,1)} %tok_ref, bf16[64,2048]{1,0:T(8,128)(2,1)} %bitcast.6, bf16[64,2048]{1,0:T(8,128)(2,1)} %bitcast.7, f32[1,64]{1,0:T(1,128)S(1)} %bitcast.4, f32[88,2048]{1,0:T(8,128)} %constant.4.clone.table_hbm), custom_call_target="tpu_custom_call" | custom-call | flops 100663296 | bytes 393216 | tf_op jit(solution)/shard_map/pallas_call | solution.py:263
  3.4 0.0 copy-start.3
  3.4 3.1 %collective-permute-start.2 = (bf16[192,128]{1,0:T(8,128)(2,1)S(1)}, bf16[192,128]{1,0:T(8,128)(2,1)S(1)}, u32[]{:S(2)}, u32[]{:S(2)}) collective-permute-start(bf16[192,128]{1,0:T(8,128)(2,1)S(1)} %shard_map.104), channel_id=1, source_target_pairs={{0,4},{4,0},{8,12},{12,8},{16,20},{20,16},{24,28},{28,24},{1,5},{5... | collective-permute-start | bytes 147464 | tf_op jit(solution)/shard_map/ppermute | solution.py:332
  6.4 2.1 %collective-permute-done.2 = bf16[192,128]{1,0:T(8,128)(2,1)S(1)} collective-permute-done((bf16[192,128]{1,0:T(8,128)(2,1)S(1)}, bf16[192,128]{1,0:T(8,128)(2,1)S(1)}, u32[]{:S(2)}, u32[]{:S(2)}) %collective-permute-start.2) | collective-permute-done | bytes 49184 | tf_op jit(solution)/shard_map/ppermute | solution.py:332
  8.5 0.0 copy-start.5
  8.5 2.1 %collective-permute-start.4 = (bf16[384,128]{1,0:T(8,128)(2,1)S(1)}, bf16[384,128]{1,0:T(8,128)(2,1)S(1)}, u32[]{:S(2)}, u32[]{:S(2)}) collective-permute-start(bf16[384,128]{1,0:T(8,128)(2,1)S(1)} %constant_dynamic-update-slice_fusion.refs_0_), channel_id=1, source_target_pairs={{0,8},{4,12},{8,0},{12,4},{16,24},{20,28},{24,16},{28,20},{1,9},{5... | collective-permute-start | bytes 294920 | tf_op jit(solution)/shard_map/ppermute | solution.py:336
  10.7 2.6 %collective-permute-start = (bf16[192,128]{1,0:T(8,128)(2,1)S(1)}, bf16[192,128]{1,0:T(8,128)(2,1)S(1)}, u32[]{:S(2)}, u32[]{:S(2)}) collective-permute-start(bf16[192,128]{1,0:T(8,128)(2,1)S(1)} %shard_map.104), channel_id=1, source_target_pairs={{0,16},{4,20},{8,24},{12,28},{16,0},{20,4},{24,8},{28,12},{1,17},{... | collective-permute-start | bytes 147464 | tf_op jit(solution)/shard_map/ppermute | solution.py:333
  13.3 0.0 collective-permute-start.3
  13.3 2.4 %collective-permute-done.refs_1_ = bf16[192,128]{1,0:T(8,128)(2,1)S(1)} collective-permute-done((bf16[192,128]{1,0:T(8,128)(2,1)S(1)}, bf16[192,128]{1,0:T(8,128)(2,1)S(1)}, u32[]{:S(2)}, u32[]{:S(2)}) %collective-permute-start) | collective-permute-done | bytes 49184 | tf_op jit(solution)/shard_map/ppermute | solution.py:333
  15.7 1.5 %collective-permute-start.1 = (bf16[192,128]{1,0:T(8,128)(2,1)S(1)}, bf16[192,128]{1,0:T(8,128)(2,1)S(1)}, u32[]{:S(2)}, u32[]{:S(2)}) collective-permute-start(bf16[192,128]{1,0:T(8,128)(2,1)S(1)} %collective-permute-done.refs_1_), channel_id=1, source_target_pairs={{0,4},{4,0},{8,12},{12,8},{16,20},{20,16},{24,28},{28,24},{1,5},{5... | collective-permute-start | bytes 147464 | tf_op jit(solution)/shard_map/ppermute | solution.py:337
  17.2 0.0 copy-done.1
  17.2 0.0 copy-done.2
  17.2 0.0 copy-done.3
  17.2 0.0 copy-done.5
  17.2 0.8 %shard_map.105.qt_ref = bf16[128,768]{1,0:T(8,128)(2,1)S(1)} custom-call(bf16[192,2048]{1,0:T(8,128)(2,1)S(1)} %copy-done.1, bf16[2048,256]{1,0:T(8,128)(2,1)S(1)} %copy-done.2, f32[1,64]{1,0:T(1,128)S(1)} %bitcast.5, f32[88,256]{1,0:T(8,128)S(1)} %copy-done.3), custom_call_target="tpu_custom_call" | custom-call | flops 201326592 | bytes 786432 | tf_op jit(solution)/shard_map/pallas_call | solution.py:288
  18.0 0.0 copy-start
  18.0 0.6 %shard_map.106 = (f32[1,768]{1,0:T(1,128)S(1)}, f32[8,768]{1,0:T(8,128)S(1)}, f32[64,768]{1,0:T(8,128)S(1)}) custom-call(bf16[128,768]{1,0:T(8,128)(2,1)S(1)} %shard_map.105.qt_ref, bf16[384,128]{1,0:T(8,128)(2,1)S(1)} %constant_dynamic-update-slice_fusion.refs_0_), custom_call_target="tpu_custom_call" | custom-call | flops 150994944 | bytes 589824 | tf_op jit(solution)/shard_map/pallas_call | solution.py:296
  18.6 0.0 collective-permute-done.4.refs_0_
  18.7 1.0 %shard_map.107 = (f32[1,768]{1,0:T(1,128)S(1)}, f32[8,768]{1,0:T(8,128)S(1)}, f32[64,768]{1,0:T(8,128)S(1)}) custom-call(bf16[128,768]{1,0:T(8,128)(2,1)S(1)} %shard_map.105.qt_ref, bf16[384,128]{1,0:T(8,128)(2,1)S(1)} %collective-permute-done.4.refs_0_, ...), custom_call_target="tpu_custom_call", output_to_operand_aliasing={{0}: (3, {}), {1}: (4, {}), {2}: (5, {})} | custom-call | flops 226492416 | bytes 884736 | tf_op jit(solution)/shard_map/pallas_call | solution.py:305
  19.7 0.1 collective-permute-done.1.refs_0_
  19.7 0.0 collective-permute-done.3.refs_1_
  19.8 0.0 copy-done
  19.8 1.4 %shard_map.108 = (bf16[192,256]{1,0:T(8,128)(2,1)S(1)}, f32[4,192]{1,0:T(4,128)S(1)}, f32[4,192]{1,0:T(4,128)S(1)}, bf16[48,2048]{1,0:T(8,128)(2,1)S(1)}) custom-call(bf16[128,768]{1,0:T(8,128)(2,1)S(1)} %shard_map.105.qt_ref, bf16[192,128]{1,0:T(8,128)(2,1)S(1)} %collective-permute-done.1.refs_0_, bf16[384,128]{1,0:T(8,128)(2,1)S(1)} %collective-permute-done.3.refs_1_, ...), custom_call_target="tpu_custom_call" | custom-call | flops 226492416 | bytes 884736 | tf_op jit(solution)/shard_map/pallas_call | solution.py:317
  21.2 0.1 collective-permute-start.6
  21.2 0.7 %shard_map.109 = (f32[48,2048]{1,0:T(8,128)S(1)}, bf16[48,2048]{1,0:T(8,128)(2,1)S(1)}, f32[48,2048]{1,0:T(8,128)S(1)}) custom-call(bf16[192,256]{1,0:T(8,128)(2,1)S(1)} %get-tuple-element.29.att_ref, bf16[256,2048]{1,0:T(8,128)(2,1)S(1)} %copy-done), custom_call_target="tpu_custom_call" | custom-call | flops 50331648 | bytes 196608 | tf_op jit(solution)/shard_map/pallas_call | solution.py:359
  21.9 0.5 %collective-permute-start.5 = (bf16[48,2048]{1,0:T(8,128)(2,1)S(1)}, bf16[48,2048]{1,0:T(8,128)(2,1)S(1)}, u32[]{:S(2)}, u32[]{:S(2)}) collective-permute-start(bf16[48,2048]{1,0:T(8,128)(2,1)S(1)} %get-tuple-element.31), channel_id=1, source_target_pairs={{0,1},{1,0},{2,3},{3,2},{4,5},{5,4},{6,7},{7,6},{8,9},{9,8},{10,11... | collective-permute-start | bytes 589832 | tf_op jit(solution)/shard_map/ppermute | solution.py:369
  22.4 0.2 collective-permute-done.6
  22.7 1.6 %collective-permute-start.7 = (bf16[48,2048]{1,0:T(8,128)(2,1)S(1)}, bf16[48,2048]{1,0:T(8,128)(2,1)S(1)}, u32[]{:S(2)}, u32[]{:S(2)}) collective-permute-start(bf16[48,2048]{1,0:T(8,128)(2,1)S(1)} %add_convert_fusion.1), channel_id=1, source_target_pairs={{0,2},{1,3},{2,0},{3,1},{4,6},{5,7},{6,4},{7,5},{8,10},{9,11},{10,... | collective-permute-start | bytes 589832 | tf_op jit(solution)/shard_map/ppermute | solution.py:369
  24.3 0.6 %log_add_fusion = f32[4,192]{1,0:T(4,128)} fusion(f32[4,192]{1,0:T(4,128)S(1)} %get-tuple-element.34, f32[4,192]{1,0:T(4,128)S(1)} %get-tuple-element.35), kind=kLoop, calls=%fused_computation.4 | loop fusion | flops 768 | bytes 9216 | tf_op jit(solution)/shard_map/add | solution.py:372
  24.9 0.0 collective-permute-done.5
  24.9 4.9 %collective-permute-done.7 = bf16[48,2048]{1,0:T(8,128)(2,1)S(1)} collective-permute-done((bf16[48,2048]{1,0:T(8,128)(2,1)S(1)}, bf16[48,2048]{1,0:T(8,128)(2,1)S(1)}, u32[]{:S(2)}, u32[]{:S(2)}) %collective-permute-start.7) | collective-permute-done | bytes 196640 | tf_op jit(solution)/shard_map/ppermute | solution.py:369
  29.7 0.8 %add_convert_fusion = bf16[48,2048]{1,0:T(8,128)(2,1)} fusion(bf16[48,2048]{1,0:T(8,128)(2,1)S(1)} %collective-permute-done.7, f32[48,2048]{1,0:T(8,128)S(1)} %get-tuple-element.30, bf16[48,2048]{1,0:T(8,128)(2,1)S(1)} %collective-permute-done.5), kind=kLoop, calls=%fused_computation | loop fusion | flops 491520 | bytes 983040 | tf_op jit(solution)/shard_map/convert_element_type | solution.py:372
  (3 shorter events, 0.1 us)
Async XLA Ops:
  0.6 0.7 %copy-start.4 = (f32[64]{0:T(128)S(1)}, f32[64]{0:T(128)}, u32[]{:S(2)}) copy-start(f32[64]{0:T(128)} %param.15) | copy-start | bytes 772
  1.3 15.9 %copy-start.1 = (bf16[192,2048]{1,0:T(8,128)(2,1)S(1)}, bf16[192,2048]{1,0:T(8,128)(2,1)}, u32[]{:S(2)}) copy-start(bf16[192,2048]{1,0:T(8,128)(2,1)} %tok_ref) | copy-start | bytes 2359300
  1.3 15.9 %copy-start.2 = (bf16[2048,256]{1,0:T(8,128)(2,1)S(1)}, bf16[2048,256]{1,0:T(8,128)(2,1)}, u32[]{:S(2)}) copy-start(bf16[2048,256]{1,0:T(8,128)(2,1)} %wq_ref) | copy-start | bytes 3145732
  3.4 13.8 %copy-start.3 = (f32[88,256]{1,0:T(8,128)S(1)}, f32[88,256]{1,0:T(8,128)}, u32[]{:S(2)}) copy-start(f32[88,256]{1,0:T(8,128)} %constant.5.clone.table_ref) | copy-start | bytes 270340
  3.4 5.1 %collective-permute-start.2 = (bf16[192,128]{1,0:T(8,128)(2,1)S(1)}, bf16[192,128]{1,0:T(8,128)(2,1)S(1)}, u32[]{:S(2)}, u32[]{:S(2)}) collective-permute-start(bf16[192,128]{1,0:T(8,128)(2,1)S(1)} %shard_map.104), channel_id=1, source_target_pairs={{0,4},{4,0},{8,12},{12,8},{16,20},{20,16},{24,28},{28,24},{1,5},{5... | collective-permute-start | bytes 147464 | tf_op jit(solution)/shard_map/ppermute | solution.py:332
  8.5 8.7 %copy-start.5 = (f32[64]{0:T(128)S(1)}, f32[64]{0:T(128)}, u32[]{:S(2)}) copy-start(f32[64]{0:T(128)} %param.14) | copy-start | bytes 772
  8.5 10.1 %collective-permute-start.4 = (bf16[384,128]{1,0:T(8,128)(2,1)S(1)}, bf16[384,128]{1,0:T(8,128)(2,1)S(1)}, u32[]{:S(2)}, u32[]{:S(2)}) collective-permute-start(bf16[384,128]{1,0:T(8,128)(2,1)S(1)} %constant_dynamic-update-slice_fusion.refs_0_), channel_id=1, source_target_pairs={{0,8},{4,12},{8,0},{12,4},{16,24},{20,28},{24,16},{28,20},{1,9},{5... | collective-permute-start | bytes 294920 | tf_op jit(solution)/shard_map/ppermute | solution.py:336
  10.7 5.0 %collective-permute-start = (bf16[192,128]{1,0:T(8,128)(2,1)S(1)}, bf16[192,128]{1,0:T(8,128)(2,1)S(1)}, u32[]{:S(2)}, u32[]{:S(2)}) collective-permute-start(bf16[192,128]{1,0:T(8,128)(2,1)S(1)} %shard_map.104), channel_id=1, source_target_pairs={{0,16},{4,20},{8,24},{12,28},{16,0},{20,4},{24,8},{28,12},{1,17},{... | collective-permute-start | bytes 147464 | tf_op jit(solution)/shard_map/ppermute | solution.py:333
  13.3 6.5 %collective-permute-start.3 = (bf16[384,128]{1,0:T(8,128)(2,1)S(1)}, bf16[384,128]{1,0:T(8,128)(2,1)S(1)}, u32[]{:S(2)}, u32[]{:S(2)}) collective-permute-start(bf16[384,128]{1,0:T(8,128)(2,1)S(1)} %constant_dynamic-update-slice_fusion.refs_0_), channel_id=1, source_target_pairs={{0,24},{4,28},{8,16},{12,20},{16,8},{20,12},{24,0},{28,4},{1,25},{... | collective-permute-start | bytes 294920 | tf_op jit(solution)/shard_map/ppermute | solution.py:335
  15.7 4.1 %collective-permute-start.1 = (bf16[192,128]{1,0:T(8,128)(2,1)S(1)}, bf16[192,128]{1,0:T(8,128)(2,1)S(1)}, u32[]{:S(2)}, u32[]{:S(2)}) collective-permute-start(bf16[192,128]{1,0:T(8,128)(2,1)S(1)} %collective-permute-done.refs_1_), channel_id=1, source_target_pairs={{0,4},{4,0},{8,12},{12,8},{16,20},{20,16},{24,28},{28,24},{1,5},{5... | collective-permute-start | bytes 147464 | tf_op jit(solution)/shard_map/ppermute | solution.py:337
  18.0 1.7 %copy-start = (bf16[256,2048]{1,0:T(8,128)(2,1)S(1)}, bf16[256,2048]{1,0:T(8,128)(2,1)}, u32[]{:S(2)}) copy-start(bf16[256,2048]{1,0:T(8,128)(2,1)} %wo_ref) | copy-start | bytes 3145732
  21.2 1.5 %collective-permute-start.6 = (bf16[48,2048]{1,0:T(8,128)(2,1)S(1)}, bf16[48,2048]{1,0:T(8,128)(2,1)S(1)}, u32[]{:S(2)}, u32[]{:S(2)}) collective-permute-start(bf16[48,2048]{1,0:T(8,128)(2,1)S(1)} %get-tuple-element.33), channel_id=1, source_target_pairs={{0,1},{1,0},{2,3},{3,2},{4,5},{5,4},{6,7},{7,6},{8,9},{9,8},{10,11... | collective-permute-start | bytes 589832 | tf_op jit(solution)/shard_map/ppermute | solution.py:369
  21.9 3.0 %collective-permute-start.5 = (bf16[48,2048]{1,0:T(8,128)(2,1)S(1)}, bf16[48,2048]{1,0:T(8,128)(2,1)S(1)}, u32[]{:S(2)}, u32[]{:S(2)}) collective-permute-start(bf16[48,2048]{1,0:T(8,128)(2,1)S(1)} %get-tuple-element.31), channel_id=1, source_target_pairs={{0,1},{1,0},{2,3},{3,2},{4,5},{5,4},{6,7},{7,6},{8,9},{9,8},{10,11... | collective-permute-start | bytes 589832 | tf_op jit(solution)/shard_map/ppermute | solution.py:369
  22.7 7.0 %collective-permute-start.7 = (bf16[48,2048]{1,0:T(8,128)(2,1)S(1)}, bf16[48,2048]{1,0:T(8,128)(2,1)S(1)}, u32[]{:S(2)}, u32[]{:S(2)}) collective-permute-start(bf16[48,2048]{1,0:T(8,128)(2,1)S(1)} %add_convert_fusion.1), channel_id=1, source_target_pairs={{0,2},{1,3},{2,0},{3,1},{4,6},{5,7},{6,4},{7,5},{8,10},{9,11},{10,... | collective-permute-start | bytes 589832 | tf_op jit(solution)/shard_map/ppermute | solution.py:369

commit v3 on v2

--- a/solution.py
+++ b/solution.py
@@ -88,8 +88,8 @@
 
 
 def kv_kernel(
-    head_dim, pieces, tok_hbm, wk_hbm, wv_hbm, gain_hbm, table_hbm,
-    out_ref, tok_ref, both_ref, gain_ref, table_ref, sems,
+    head_dim, pieces, tok_hbm, wk_hbm, wv_hbm, gain_ref, table_hbm,
+    out_ref, tok_ref, both_ref, table_ref, sems,
 ):
     rows, width = tok_ref.shape
     step = width // pieces
@@ -99,7 +99,6 @@
         copies.start(tok_hbm.at[:, part], tok_ref.at[:, part])
         copies.start(wk_hbm.at[:, part], both_ref.at[pl.ds(0, head_dim), part])
         copies.start(wv_hbm.at[:, part], both_ref.at[pl.ds(head_dim, head_dim), part])
-    copies.start(gain_hbm, gain_ref)
     copies.start(table_hbm.at[:, pl.ds(0, 2 * LANES)], table_ref)
     raw = None
     for i in range(pieces):
@@ -112,38 +111,38 @@
     raw = raw.astype(jnp.bfloat16).astype(jnp.float32)
     lane = lax.broadcasted_iota(jnp.int32, (1, LANES), 1)
     row_start = lax.axis_index("sp") * (rows // GRID_W)
-    copies.wait(3 * pieces, 3 * pieces + 2)
+    copies.wait(3 * pieces, 3 * pieces + 1)
     keys = turn(normed(raw, gain_ref[...], head_dim), row_start, table_ref, head_dim)
     out_ref[...] = jnp.where(lane < head_dim, keys, raw).astype(jnp.bfloat16)
 
 
 def attend(qt, kvs, head_dim, top, total, acc, score_ref, weight_ref):
     width = qt.shape[1]
-    count = 0
-    eight = None
-    values = []
+    states = [] if top is None else [(top, total, acc)]
+    at = 0
     for kv in kvs:
-        scores = jnp.dot(kv, qt, preferred_element_type=jnp.float32)
-        score_ref[count : count + kv.shape[0], :] = scores
-        for i in range(0, kv.shape[0], 8):
-            most = score_ref[count + i : count + i + 8, :]
-            eight = most if eight is None else jnp.maximum(eight, most)
-        values.append(kv.astype(jnp.float32).T[head_dim : 2 * head_dim].astype(jnp.bfloat16))
-        count += kv.shape[0]
-    new_top = jnp.max(eight, axis=0, keepdims=True)
-    if top is not None:
-        new_top = jnp.maximum(top, new_top)
-    part = jnp.zeros((8, width), jnp.float32)
-    for at in range(0, count, 16):
-        expos = jnp.exp(score_ref[at : at + 16, :] - new_top)
-        weight_ref[at : at + 16, :] = expos.astype(jnp.bfloat16)
-        part = part + (expos[:8] + expos[8:])
-    values = jnp.concatenate(values, axis=1)
-    fresh = jnp.dot(values, weight_ref[0:count, :], preferred_element_type=jnp.float32)
-    if top is None:
-        return new_top, part, fresh
-    shrink = jnp.exp(top - new_top)
-    return new_top, total * shrink + part, acc * shrink + fresh
+        count = kv.shape[0]
+        score_ref[at : at + count, :] = jnp.dot(kv, qt, preferred_element_type=jnp.float32)
+        eight = score_ref[at : at + 8, :]
+        for i in range(8, count, 8):
+            eight = jnp.maximum(eight, score_ref[at + i : at + i + 8, :])
+        most = jnp.max(eight, axis=0, keepdims=True)
+        part = jnp.zeros((8, width), jnp.float32)
+        for i in range(at, at + count, 16):
+            expos = jnp.exp(score_ref[i : i + 16, :] - most)
+            weight_ref[i : i + 16, :] = expos.astype(jnp.bfloat16)
+            part = part + (expos[:8] + expos[8:])
+        values = kv.astype(jnp.float32).T[head_dim : 2 * head_dim].astype(jnp.bfloat16)
+        weights = weight_ref[at : at + count, :]
+        states.append((most, part, jnp.dot(values, weights, preferred_element_type=jnp.float32)))
+        at += count
+    if len(states) == 1:
+        return states[0]
+    top = functools.reduce(jnp.maximum, [state[0] for state in states])
+    shrinks = [jnp.exp(state[0] - top) for state in states]
+    total = sum(state[1] * shrink for state, shrink in zip(states, shrinks))
+    acc = sum(state[2] * shrink for state, shrink in zip(states, shrinks))
+    return top, total, acc
 
 
 def attend_all(qt_ref, kv_refs, head_dim, state, score_ref, weight_ref):
@@ -264,13 +263,13 @@
         functools.partial(kv_kernel, head_dim, pieces),
         bf16((rows, LANES)),
         2 * rows * width * LANES,
-        [HBM] * 5,
+        [HBM] * 3 + [VMEM, HBM],
         KV_LIMIT,
         scratch_shapes=[
             pltpu.VMEM(tokens.shape, jnp.bfloat16),
             pltpu.VMEM((LANES, width), jnp.bfloat16),
-            *scratch,
-            pltpu.SemaphoreType.DMA((3 * pieces + 2,)),
+            scratch[1],
+            pltpu.SemaphoreType.DMA((3 * pieces + 1,)),
         ],
     )(tokens, w_key.T, w_value.T, key_gain[None, :], wide)
 

time: 30.6 us -> 30.6 us (level)
  no operation moved by 1% of the time
where the time goes in v3:
time: 30.6 us; the launch traced here: 30.4 us
  starting transfers between devices  11.5 us (38%)
  waiting for transfers between devices  9.7 us (32%)
  Pallas kernels  6.42 us (21%)
  other arithmetic  1.39 us (5%)
  between operations  0.73 us (2%)
  local copies, waits for them, and re-layouts  0.69 us (2%)
    ppermute x3, waiting for transfers between devices, shards(): lax.ppermute(parts[d + bit].astype(jnp.bfloat16), 'tp', xor(n_tp, bit))  5.09 us
    ppermute x1, starting transfers between devices, shards(): near = send(kv, perm=xor(n_sp, 1))  3.06 us
    ppermute x1, starting transfers between devices, shards(): far = send(kv, perm=xor(n_sp, 4))  2.59 us
    ppermute x1, waiting for transfers between devices, shards(): far = send(kv, perm=xor(n_sp, 4))  2.4 us
    ppermute x3, starting transfers between devices, shards(): lax.ppermute(parts[d + bit].astype(jnp.bfloat16), 'tp', xor(n_tp, bit))  2.16 us
    ppermute x1, starting transfers between devices, shards(): beside = send(pair, perm=xor(n_sp, 2))  2.15 us
    ppermute x1, waiting for transfers between devices, shards(): near = send(kv, perm=xor(n_sp, 1))  2.06 us
    pallas_call x1, Pallas kernels, shards(): call(functools.partial(kv_kernel, head_dim, pieces), bf16((rows, LANES)),...  2.05 us
  transfers between devices with their start and end apart: 8, of which 5 were waited for; matrix products, arithmetic and copies ran while one was open for 2% of the time, Pallas kernels for 10%

profile of v3, /device:TPU:0, one launch (start us, length us, event | category | flops | bytes accessed | tf_op | source)
XLA Modules:
  0.0 30.4 jit_solution(15294583100375000980)
XLA Ops:
  0.6 0.0 copy-start.4
  0.6 0.6 %copy-done.4 = f32[64]{0:T(128)S(1)} copy-done((f32[64]{0:T(128)S(1)}, f32[64]{0:T(128)}, u32[]{:S(2)}) %copy-start.4) | copy-done | bytes 280
  1.3 0.0 copy-start.1
  1.3 0.0 copy-start.2
  1.3 2.0 %shard_map.104 = bf16[192,128]{1,0:T(8,128)(2,1)S(1)} custom-call(bf16[192,2048]{1,0:T(8,128)(2,1)} %tok_ref, bf16[64,2048]{1,0:T(8,128)(2,1)} %bitcast.6, bf16[64,2048]{1,0:T(8,128)(2,1)} %bitcast.7, f32[1,64]{1,0:T(1,128)S(1)} %bitcast.4, f32[88,2048]{1,0:T(8,128)} %constant.4.clone.table_hbm), custom_call_target="tpu_custom_call" | custom-call | flops 100663296 | bytes 393216 | tf_op jit(solution)/shard_map/pallas_call | solution.py:262
  3.3 0.0 copy-start.3
  3.4 3.1 %collective-permute-start.2 = (bf16[192,128]{1,0:T(8,128)(2,1)S(1)}, bf16[192,128]{1,0:T(8,128)(2,1)S(1)}, u32[]{:S(2)}, u32[]{:S(2)}) collective-permute-start(bf16[192,128]{1,0:T(8,128)(2,1)S(1)} %shard_map.104), channel_id=1, source_target_pairs={{0,4},{4,0},{8,12},{12,8},{16,20},{20,16},{24,28},{28,24},{1,5},{5... | collective-permute-start | bytes 147464 | tf_op jit(solution)/shard_map/ppermute | solution.py:331
  6.4 2.1 %collective-permute-done.2 = bf16[192,128]{1,0:T(8,128)(2,1)S(1)} collective-permute-done((bf16[192,128]{1,0:T(8,128)(2,1)S(1)}, bf16[192,128]{1,0:T(8,128)(2,1)S(1)}, u32[]{:S(2)}, u32[]{:S(2)}) %collective-permute-start.2) | collective-permute-done | bytes 49184 | tf_op jit(solution)/shard_map/ppermute | solution.py:331
  8.5 0.0 copy-start.5
  8.5 2.1 %collective-permute-start.4 = (bf16[384,128]{1,0:T(8,128)(2,1)S(1)}, bf16[384,128]{1,0:T(8,128)(2,1)S(1)}, u32[]{:S(2)}, u32[]{:S(2)}) collective-permute-start(bf16[384,128]{1,0:T(8,128)(2,1)S(1)} %constant_dynamic-update-slice_fusion.refs_0_), channel_id=1, source_target_pairs={{0,8},{4,12},{8,0},{12,4},{16,24},{20,28},{24,16},{28,20},{1,9},{5... | collective-permute-start | bytes 294920 | tf_op jit(solution)/shard_map/ppermute | solution.py:335
  10.7 2.6 %collective-permute-start = (bf16[192,128]{1,0:T(8,128)(2,1)S(1)}, bf16[192,128]{1,0:T(8,128)(2,1)S(1)}, u32[]{:S(2)}, u32[]{:S(2)}) collective-permute-start(bf16[192,128]{1,0:T(8,128)(2,1)S(1)} %shard_map.104), channel_id=1, source_target_pairs={{0,16},{4,20},{8,24},{12,28},{16,0},{20,4},{24,8},{28,12},{1,17},{... | collective-permute-start | bytes 147464 | tf_op jit(solution)/shard_map/ppermute | solution.py:332
  13.2 0.0 collective-permute-start.3
  13.2 2.4 %collective-permute-done.refs_1_ = bf16[192,128]{1,0:T(8,128)(2,1)S(1)} collective-permute-done((bf16[192,128]{1,0:T(8,128)(2,1)S(1)}, bf16[192,128]{1,0:T(8,128)(2,1)S(1)}, u32[]{:S(2)}, u32[]{:S(2)}) %collective-permute-start) | collective-permute-done | bytes 49184 | tf_op jit(solution)/shard_map/ppermute | solution.py:332
  15.6 1.5 %collective-permute-start.1 = (bf16[192,128]{1,0:T(8,128)(2,1)S(1)}, bf16[192,128]{1,0:T(8,128)(2,1)S(1)}, u32[]{:S(2)}, u32[]{:S(2)}) collective-permute-start(bf16[192,128]{1,0:T(8,128)(2,1)S(1)} %collective-permute-done.refs_1_), channel_id=1, source_target_pairs={{0,4},{4,0},{8,12},{12,8},{16,20},{20,16},{24,28},{28,24},{1,5},{5... | collective-permute-start | bytes 147464 | tf_op jit(solution)/shard_map/ppermute | solution.py:336
  17.2 0.0 copy-done.1
  17.2 0.0 copy-done.2
  17.2 0.0 copy-done.3
  17.2 0.0 copy-done.5
  17.2 0.8 %shard_map.105.qt_ref = bf16[128,768]{1,0:T(8,128)(2,1)S(1)} custom-call(bf16[192,2048]{1,0:T(8,128)(2,1)S(1)} %copy-done.1, bf16[2048,256]{1,0:T(8,128)(2,1)S(1)} %copy-done.2, f32[1,64]{1,0:T(1,128)S(1)} %bitcast.5, f32[88,256]{1,0:T(8,128)S(1)} %copy-done.3), custom_call_target="tpu_custom_call" | custom-call | flops 201326592 | bytes 786432 | tf_op jit(solution)/shard_map/pallas_call | solution.py:287
  18.0 0.0 copy-start
  18.0 0.6 %shard_map.106 = (f32[1,768]{1,0:T(1,128)S(1)}, f32[8,768]{1,0:T(8,128)S(1)}, f32[64,768]{1,0:T(8,128)S(1)}) custom-call(bf16[128,768]{1,0:T(8,128)(2,1)S(1)} %shard_map.105.qt_ref, bf16[384,128]{1,0:T(8,128)(2,1)S(1)} %constant_dynamic-update-slice_fusion.refs_0_), custom_call_target="tpu_custom_call" | custom-call | flops 150994944 | bytes 589824 | tf_op jit(solution)/shard_map/pallas_call | solution.py:295
  18.6 0.0 collective-permute-done.4.refs_0_
  18.6 0.9 %shard_map.107 = (f32[1,768]{1,0:T(1,128)S(1)}, f32[8,768]{1,0:T(8,128)S(1)}, f32[64,768]{1,0:T(8,128)S(1)}) custom-call(bf16[128,768]{1,0:T(8,128)(2,1)S(1)} %shard_map.105.qt_ref, bf16[384,128]{1,0:T(8,128)(2,1)S(1)} %collective-permute-done.4.refs_0_, ...), custom_call_target="tpu_custom_call", output_to_operand_aliasing={{0}: (3, {}), {1}: (4, {}), {2}: (5, {})} | custom-call | flops 226492416 | bytes 884736 | tf_op jit(solution)/shard_map/pallas_call | solution.py:304
  19.6 0.1 collective-permute-done.1.refs_0_
  19.7 0.0 collective-permute-done.3.refs_1_
  19.7 0.0 copy-done
  19.7 1.3 %shard_map.108 = (bf16[192,256]{1,0:T(8,128)(2,1)S(1)}, f32[4,192]{1,0:T(4,128)S(1)}, f32[4,192]{1,0:T(4,128)S(1)}, bf16[48,2048]{1,0:T(8,128)(2,1)S(1)}) custom-call(bf16[128,768]{1,0:T(8,128)(2,1)S(1)} %shard_map.105.qt_ref, bf16[192,128]{1,0:T(8,128)(2,1)S(1)} %collective-permute-done.1.refs_0_, bf16[384,128]{1,0:T(8,128)(2,1)S(1)} %collective-permute-done.3.refs_1_, ...), custom_call_target="tpu_custom_call" | custom-call | flops 226492416 | bytes 884736 | tf_op jit(solution)/shard_map/pallas_call | solution.py:316
  21.1 0.1 collective-permute-start.6
  21.2 0.7 %shard_map.109 = (f32[48,2048]{1,0:T(8,128)S(1)}, bf16[48,2048]{1,0:T(8,128)(2,1)S(1)}, f32[48,2048]{1,0:T(8,128)S(1)}) custom-call(bf16[192,256]{1,0:T(8,128)(2,1)S(1)} %get-tuple-element.29.att_ref, bf16[256,2048]{1,0:T(8,128)(2,1)S(1)} %copy-done), custom_call_target="tpu_custom_call" | custom-call | flops 50331648 | bytes 196608 | tf_op jit(solution)/shard_map/pallas_call | solution.py:358
  21.8 0.5 %collective-permute-start.5 = (bf16[48,2048]{1,0:T(8,128)(2,1)S(1)}, bf16[48,2048]{1,0:T(8,128)(2,1)S(1)}, u32[]{:S(2)}, u32[]{:S(2)}) collective-permute-start(bf16[48,2048]{1,0:T(8,128)(2,1)S(1)} %get-tuple-element.31), channel_id=1, source_target_pairs={{0,1},{1,0},{2,3},{3,2},{4,5},{5,4},{6,7},{7,6},{8,9},{9,8},{10,11... | collective-permute-start | bytes 589832 | tf_op jit(solution)/shard_map/ppermute | solution.py:368
  22.4 0.2 collective-permute-done.6
  22.6 1.6 %collective-permute-start.7 = (bf16[48,2048]{1,0:T(8,128)(2,1)S(1)}, bf16[48,2048]{1,0:T(8,128)(2,1)S(1)}, u32[]{:S(2)}, u32[]{:S(2)}) collective-permute-start(bf16[48,2048]{1,0:T(8,128)(2,1)S(1)} %add_convert_fusion.1), channel_id=1, source_target_pairs={{0,2},{1,3},{2,0},{3,1},{4,6},{5,7},{6,4},{7,5},{8,10},{9,11},{10,... | collective-permute-start | bytes 589832 | tf_op jit(solution)/shard_map/ppermute | solution.py:368
  24.2 0.6 %log_add_fusion = f32[4,192]{1,0:T(4,128)} fusion(f32[4,192]{1,0:T(4,128)S(1)} %get-tuple-element.34, f32[4,192]{1,0:T(4,128)S(1)} %get-tuple-element.35), kind=kLoop, calls=%fused_computation.4 | loop fusion | flops 768 | bytes 9216 | tf_op jit(solution)/shard_map/add | solution.py:371
  24.8 0.0 collective-permute-done.5
  24.8 4.9 %collective-permute-done.7 = bf16[48,2048]{1,0:T(8,128)(2,1)S(1)} collective-permute-done((bf16[48,2048]{1,0:T(8,128)(2,1)S(1)}, bf16[48,2048]{1,0:T(8,128)(2,1)S(1)}, u32[]{:S(2)}, u32[]{:S(2)}) %collective-permute-start.7) | collective-permute-done | bytes 196640 | tf_op jit(solution)/shard_map/ppermute | solution.py:368
  29.7 0.8 %add_convert_fusion = bf16[48,2048]{1,0:T(8,128)(2,1)} fusion(bf16[48,2048]{1,0:T(8,128)(2,1)S(1)} %collective-permute-done.7, f32[48,2048]{1,0:T(8,128)S(1)} %get-tuple-element.30, bf16[48,2048]{1,0:T(8,128)(2,1)S(1)} %collective-permute-done.5), kind=kLoop, calls=%fused_computation | loop fusion | flops 491520 | bytes 983040 | tf_op jit(solution)/shard_map/convert_element_type | solution.py:371
  (3 shorter events, 0.1 us)
Async XLA Ops:
  0.6 0.7 %copy-start.4 = (f32[64]{0:T(128)S(1)}, f32[64]{0:T(128)}, u32[]{:S(2)}) copy-start(f32[64]{0:T(128)} %param.15) | copy-start | bytes 772
  1.3 15.9 %copy-start.1 = (bf16[192,2048]{1,0:T(8,128)(2,1)S(1)}, bf16[192,2048]{1,0:T(8,128)(2,1)}, u32[]{:S(2)}) copy-start(bf16[192,2048]{1,0:T(8,128)(2,1)} %tok_ref) | copy-start | bytes 2359300
  1.3 15.9 %copy-start.2 = (bf16[2048,256]{1,0:T(8,128)(2,1)S(1)}, bf16[2048,256]{1,0:T(8,128)(2,1)}, u32[]{:S(2)}) copy-start(bf16[2048,256]{1,0:T(8,128)(2,1)} %wq_ref) | copy-start | bytes 3145732
  3.3 13.8 %copy-start.3 = (f32[88,256]{1,0:T(8,128)S(1)}, f32[88,256]{1,0:T(8,128)}, u32[]{:S(2)}) copy-start(f32[88,256]{1,0:T(8,128)} %constant.5.clone.table_ref) | copy-start | bytes 270340
  3.4 5.1 %collective-permute-start.2 = (bf16[192,128]{1,0:T(8,128)(2,1)S(1)}, bf16[192,128]{1,0:T(8,128)(2,1)S(1)}, u32[]{:S(2)}, u32[]{:S(2)}) collective-permute-start(bf16[192,128]{1,0:T(8,128)(2,1)S(1)} %shard_map.104), channel_id=1, source_target_pairs={{0,4},{4,0},{8,12},{12,8},{16,20},{20,16},{24,28},{28,24},{1,5},{5... | collective-permute-start | bytes 147464 | tf_op jit(solution)/shard_map/ppermute | solution.py:331
  8.5 8.7 %copy-start.5 = (f32[64]{0:T(128)S(1)}, f32[64]{0:T(128)}, u32[]{:S(2)}) copy-start(f32[64]{0:T(128)} %param.14) | copy-start | bytes 772
  8.5 10.1 %collective-permute-start.4 = (bf16[384,128]{1,0:T(8,128)(2,1)S(1)}, bf16[384,128]{1,0:T(8,128)(2,1)S(1)}, u32[]{:S(2)}, u32[]{:S(2)}) collective-permute-start(bf16[384,128]{1,0:T(8,128)(2,1)S(1)} %constant_dynamic-update-slice_fusion.refs_0_), channel_id=1, source_target_pairs={{0,8},{4,12},{8,0},{12,4},{16,24},{20,28},{24,16},{28,20},{1,9},{5... | collective-permute-start | bytes 294920 | tf_op jit(solution)/shard_map/ppermute | solution.py:335
  10.7 5.0 %collective-permute-start = (bf16[192,128]{1,0:T(8,128)(2,1)S(1)}, bf16[192,128]{1,0:T(8,128)(2,1)S(1)}, u32[]{:S(2)}, u32[]{:S(2)}) collective-permute-start(bf16[192,128]{1,0:T(8,128)(2,1)S(1)} %shard_map.104), channel_id=1, source_target_pairs={{0,16},{4,20},{8,24},{12,28},{16,0},{20,4},{24,8},{28,12},{1,17},{... | collective-permute-start | bytes 147464 | tf_op jit(solution)/shard_map/ppermute | solution.py:332
  13.2 6.5 %collective-permute-start.3 = (bf16[384,128]{1,0:T(8,128)(2,1)S(1)}, bf16[384,128]{1,0:T(8,128)(2,1)S(1)}, u32[]{:S(2)}, u32[]{:S(2)}) collective-permute-start(bf16[384,128]{1,0:T(8,128)(2,1)S(1)} %constant_dynamic-update-slice_fusion.refs_0_), channel_id=1, source_target_pairs={{0,24},{4,28},{8,16},{12,20},{16,8},{20,12},{24,0},{28,4},{1,25},{... | collective-permute-start | bytes 294920 | tf_op jit(solution)/shard_map/ppermute | solution.py:334
  15.6 4.1 %collective-permute-start.1 = (bf16[192,128]{1,0:T(8,128)(2,1)S(1)}, bf16[192,128]{1,0:T(8,128)(2,1)S(1)}, u32[]{:S(2)}, u32[]{:S(2)}) collective-permute-start(bf16[192,128]{1,0:T(8,128)(2,1)S(1)} %collective-permute-done.refs_1_), channel_id=1, source_target_pairs={{0,4},{4,0},{8,12},{12,8},{16,20},{20,16},{24,28},{28,24},{1,5},{5... | collective-permute-start | bytes 147464 | tf_op jit(solution)/shard_map/ppermute | solution.py:336
  18.0 1.7 %copy-start = (bf16[256,2048]{1,0:T(8,128)(2,1)S(1)}, bf16[256,2048]{1,0:T(8,128)(2,1)}, u32[]{:S(2)}) copy-start(bf16[256,2048]{1,0:T(8,128)(2,1)} %wo_ref) | copy-start | bytes 3145732
  21.1 1.5 %collective-permute-start.6 = (bf16[48,2048]{1,0:T(8,128)(2,1)S(1)}, bf16[48,2048]{1,0:T(8,128)(2,1)S(1)}, u32[]{:S(2)}, u32[]{:S(2)}) collective-permute-start(bf16[48,2048]{1,0:T(8,128)(2,1)S(1)} %get-tuple-element.33), channel_id=1, source_target_pairs={{0,1},{1,0},{2,3},{3,2},{4,5},{5,4},{6,7},{7,6},{8,9},{9,8},{10,11... | collective-permute-start | bytes 589832 | tf_op jit(solution)/shard_map/ppermute | solution.py:368
  21.8 3.0 %collective-permute-start.5 = (bf16[48,2048]{1,0:T(8,128)(2,1)S(1)}, bf16[48,2048]{1,0:T(8,128)(2,1)S(1)}, u32[]{:S(2)}, u32[]{:S(2)}) collective-permute-start(bf16[48,2048]{1,0:T(8,128)(2,1)S(1)} %get-tuple-element.31), channel_id=1, source_target_pairs={{0,1},{1,0},{2,3},{3,2},{4,5},{5,4},{6,7},{7,6},{8,9},{9,8},{10,11... | collective-permute-start | bytes 589832 | tf_op jit(solution)/shard_map/ppermute | solution.py:368
  22.6 7.0 %collective-permute-start.7 = (bf16[48,2048]{1,0:T(8,128)(2,1)S(1)}, bf16[48,2048]{1,0:T(8,128)(2,1)S(1)}, u32[]{:S(2)}, u32[]{:S(2)}) collective-permute-start(bf16[48,2048]{1,0:T(8,128)(2,1)S(1)} %add_convert_fusion.1), channel_id=1, source_target_pairs={{0,2},{1,3},{2,0},{3,1},{4,6},{5,7},{6,4},{7,5},{8,10},{9,11},{10,... | collective-permute-start | bytes 589832 | tf_op jit(solution)/shard_map/ppermute | solution.py:368

commit v4 on v3

--- a/solution.py
+++ b/solution.py
@@ -108,12 +108,30 @@
             tok_ref[:, part], both_ref[:, part], NT, preferred_element_type=jnp.float32
         )
         raw = more if raw is None else raw + more
-    raw = raw.astype(jnp.bfloat16).astype(jnp.float32)
+    rounded = raw.astype(jnp.bfloat16)
+    quarter = head_dim // 4
+    source = lax.broadcasted_iota(jnp.int32, (LANES, LANES), 0)
+    target = lax.broadcasted_iota(jnp.int32, (LANES, LANES), 1)
+    step = jnp.where(target % (2 * quarter) < quarter, quarter, -quarter)
+    swap = jnp.where(source == target + step, 1.0, 0.0).astype(jnp.bfloat16)
+    other = jnp.dot(rounded, swap, preferred_element_type=jnp.float32)
+    raw = rounded.astype(jnp.float32)
     lane = lax.broadcasted_iota(jnp.int32, (1, LANES), 1)
+    mine = lane < head_dim
+    mean = jnp.sum(jnp.where(mine, raw * raw, 0.0), axis=1, keepdims=True) * (1.0 / head_dim)
+    scale = lax.rsqrt(mean + NORM_EPS)
+    gain = jnp.concatenate([gain_ref[...]] * (LANES // head_dim), axis=1)
+    ahead, behind = pltpu.roll(gain, LANES - quarter, 1), pltpu.roll(gain, quarter, 1)
+    other_gain = jnp.where(lane % (2 * quarter) < quarter, ahead, behind)
     row_start = lax.axis_index("sp") * (rows // GRID_W)
     copies.wait(3 * pieces, 3 * pieces + 1)
-    keys = turn(normed(raw, gain_ref[...], head_dim), row_start, table_ref, head_dim)
-    out_ref[...] = jnp.where(lane < head_dim, keys, raw).astype(jnp.bfloat16)
+    columns = table_ref[0:GRID_W, :]
+    for j in range(rows // GRID_W):
+        part = slice(j * GRID_W, (j + 1) * GRID_W)
+        both = columns + table_ref[pl.ds(GRID_W + row_start + j, 1), :]
+        keys = raw[part] * (gain * both[:, :LANES]) + other[part] * (other_gain * both[:, LANES:])
+        out = jnp.where(mine, keys * scale[part], raw[part])
+        out_ref[part, :] = out.astype(jnp.bfloat16)
 
 
 def attend(qt, kvs, head_dim, top, total, acc, score_ref, weight_ref):

time: 30.6 us -> 30.5 us (level)
  no operation moved by 1% of the time
where the time goes in v4:
time: 30.5 us; the launch traced here: 30.3 us
  starting transfers between devices  11.5 us (38%)
  waiting for transfers between devices  9.68 us (32%)
  Pallas kernels  6.36 us (21%)
  other arithmetic  1.39 us (5%)
  between operations  0.73 us (2%)
  local copies, waits for them, and re-layouts  0.69 us (2%)
    ppermute x3, waiting for transfers between devices, shards(): lax.ppermute(parts[d + bit].astype(jnp.bfloat16), 'tp', xor(n_tp, bit))  5.08 us
    ppermute x1, starting transfers between devices, shards(): near = send(kv, perm=xor(n_sp, 1))  3.07 us
    ppermute x1, starting transfers between devices, shards(): far = send(kv, perm=xor(n_sp, 4))  2.59 us
    ppermute x1, waiting for transfers between devices, shards(): far = send(kv, perm=xor(n_sp, 4))  2.39 us
    ppermute x3, starting transfers between devices, shards(): lax.ppermute(parts[d + bit].astype(jnp.bfloat16), 'tp', xor(n_tp, bit))  2.16 us
    ppermute x1, starting transfers between devices, shards(): beside = send(pair, perm=xor(n_sp, 2))  2.14 us
    ppermute x1, waiting for transfers between devices, shards(): near = send(kv, perm=xor(n_sp, 1))  2.06 us
    pallas_call x1, Pallas kernels, shards(): call(functools.partial(kv_kernel, head_dim, pieces), bf16((rows, LANES)),...  1.98 us
  transfers between devices with their start and end apart: 8, of which 5 were waited for; matrix products, arithmetic and copies ran while one was open for 2% of the time, Pallas kernels for 10%

profile of v4, /device:TPU:0, one launch (start us, length us, event | category | flops | bytes accessed | tf_op | source)
XLA Modules:
  0.0 30.3 jit_solution(5805755395195107231)
XLA Ops:
  0.6 0.0 copy-start.4
  0.6 0.6 %copy-done.4 = f32[64]{0:T(128)S(1)} copy-done((f32[64]{0:T(128)S(1)}, f32[64]{0:T(128)}, u32[]{:S(2)}) %copy-start.4) | copy-done | bytes 280
  1.3 0.0 copy-start.1
  1.3 0.0 copy-start.2
  1.3 2.0 %shard_map.104 = bf16[192,128]{1,0:T(8,128)(2,1)S(1)} custom-call(bf16[192,2048]{1,0:T(8,128)(2,1)} %tok_ref, bf16[64,2048]{1,0:T(8,128)(2,1)} %bitcast.6, bf16[64,2048]{1,0:T(8,128)(2,1)} %bitcast.7, f32[1,64]{1,0:T(1,128)S(1)} %bitcast.4, f32[88,2048]{1,0:T(8,128)} %constant.4.clone.table_hbm), custom_call_target="tpu_custom_call" | custom-call | flops 100663296 | bytes 393216 | tf_op jit(solution)/shard_map/pallas_call | solution.py:280
  3.3 0.0 copy-start.3
  3.3 3.1 %collective-permute-start.2 = (bf16[192,128]{1,0:T(8,128)(2,1)S(1)}, bf16[192,128]{1,0:T(8,128)(2,1)S(1)}, u32[]{:S(2)}, u32[]{:S(2)}) collective-permute-start(bf16[192,128]{1,0:T(8,128)(2,1)S(1)} %shard_map.104), channel_id=1, source_target_pairs={{0,4},{4,0},{8,12},{12,8},{16,20},{20,16},{24,28},{28,24},{1,5},{5... | collective-permute-start | bytes 147464 | tf_op jit(solution)/shard_map/ppermute | solution.py:349
  6.4 2.1 %collective-permute-done.2 = bf16[192,128]{1,0:T(8,128)(2,1)S(1)} collective-permute-done((bf16[192,128]{1,0:T(8,128)(2,1)S(1)}, bf16[192,128]{1,0:T(8,128)(2,1)S(1)}, u32[]{:S(2)}, u32[]{:S(2)}) %collective-permute-start.2) | collective-permute-done | bytes 49184 | tf_op jit(solution)/shard_map/ppermute | solution.py:349
  8.4 0.0 copy-start.5
  8.4 2.1 %collective-permute-start.4 = (bf16[384,128]{1,0:T(8,128)(2,1)S(1)}, bf16[384,128]{1,0:T(8,128)(2,1)S(1)}, u32[]{:S(2)}, u32[]{:S(2)}) collective-permute-start(bf16[384,128]{1,0:T(8,128)(2,1)S(1)} %constant_dynamic-update-slice_fusion.refs_0_), channel_id=1, source_target_pairs={{0,8},{4,12},{8,0},{12,4},{16,24},{20,28},{24,16},{28,20},{1,9},{5... | collective-permute-start | bytes 294920 | tf_op jit(solution)/shard_map/ppermute | solution.py:353
  10.6 2.6 %collective-permute-start = (bf16[192,128]{1,0:T(8,128)(2,1)S(1)}, bf16[192,128]{1,0:T(8,128)(2,1)S(1)}, u32[]{:S(2)}, u32[]{:S(2)}) collective-permute-start(bf16[192,128]{1,0:T(8,128)(2,1)S(1)} %shard_map.104), channel_id=1, source_target_pairs={{0,16},{4,20},{8,24},{12,28},{16,0},{20,4},{24,8},{28,12},{1,17},{... | collective-permute-start | bytes 147464 | tf_op jit(solution)/shard_map/ppermute | solution.py:350
  13.2 0.0 collective-permute-start.3
  13.2 2.4 %collective-permute-done.refs_1_ = bf16[192,128]{1,0:T(8,128)(2,1)S(1)} collective-permute-done((bf16[192,128]{1,0:T(8,128)(2,1)S(1)}, bf16[192,128]{1,0:T(8,128)(2,1)S(1)}, u32[]{:S(2)}, u32[]{:S(2)}) %collective-permute-start) | collective-permute-done | bytes 49184 | tf_op jit(solution)/shard_map/ppermute | solution.py:350
  15.6 1.5 %collective-permute-start.1 = (bf16[192,128]{1,0:T(8,128)(2,1)S(1)}, bf16[192,128]{1,0:T(8,128)(2,1)S(1)}, u32[]{:S(2)}, u32[]{:S(2)}) collective-permute-start(bf16[192,128]{1,0:T(8,128)(2,1)S(1)} %collective-permute-done.refs_1_), channel_id=1, source_target_pairs={{0,4},{4,0},{8,12},{12,8},{16,20},{20,16},{24,28},{28,24},{1,5},{5... | collective-permute-start | bytes 147464 | tf_op jit(solution)/shard_map/ppermute | solution.py:354
  17.1 0.0 copy-done.1
  17.1 0.0 copy-done.2
  17.1 0.0 copy-done.3
  17.1 0.0 copy-done.5
  17.1 0.8 %shard_map.105.qt_ref = bf16[128,768]{1,0:T(8,128)(2,1)S(1)} custom-call(bf16[192,2048]{1,0:T(8,128)(2,1)S(1)} %copy-done.1, bf16[2048,256]{1,0:T(8,128)(2,1)S(1)} %copy-done.2, f32[1,64]{1,0:T(1,128)S(1)} %bitcast.5, f32[88,256]{1,0:T(8,128)S(1)} %copy-done.3), custom_call_target="tpu_custom_call" | custom-call | flops 201326592 | bytes 786432 | tf_op jit(solution)/shard_map/pallas_call | solution.py:305
  17.9 0.0 copy-start
  17.9 0.6 %shard_map.106 = (f32[1,768]{1,0:T(1,128)S(1)}, f32[8,768]{1,0:T(8,128)S(1)}, f32[64,768]{1,0:T(8,128)S(1)}) custom-call(bf16[128,768]{1,0:T(8,128)(2,1)S(1)} %shard_map.105.qt_ref, bf16[384,128]{1,0:T(8,128)(2,1)S(1)} %constant_dynamic-update-slice_fusion.refs_0_), custom_call_target="tpu_custom_call" | custom-call | flops 150994944 | bytes 589824 | tf_op jit(solution)/shard_map/pallas_call | solution.py:313
  18.6 0.0 collective-permute-done.4.refs_0_
  18.6 0.9 %shard_map.107 = (f32[1,768]{1,0:T(1,128)S(1)}, f32[8,768]{1,0:T(8,128)S(1)}, f32[64,768]{1,0:T(8,128)S(1)}) custom-call(bf16[128,768]{1,0:T(8,128)(2,1)S(1)} %shard_map.105.qt_ref, bf16[384,128]{1,0:T(8,128)(2,1)S(1)} %collective-permute-done.4.refs_0_, ...), custom_call_target="tpu_custom_call", output_to_operand_aliasing={{0}: (3, {}), {1}: (4, {}), {2}: (5, {})} | custom-call | flops 226492416 | bytes 884736 | tf_op jit(solution)/shard_map/pallas_call | solution.py:322
  19.5 0.1 collective-permute-done.1.refs_0_
  19.7 0.0 collective-permute-done.3.refs_1_
  19.7 0.0 copy-done
  19.7 1.3 %shard_map.108 = (bf16[192,256]{1,0:T(8,128)(2,1)S(1)}, f32[4,192]{1,0:T(4,128)S(1)}, f32[4,192]{1,0:T(4,128)S(1)}, bf16[48,2048]{1,0:T(8,128)(2,1)S(1)}) custom-call(bf16[128,768]{1,0:T(8,128)(2,1)S(1)} %shard_map.105.qt_ref, bf16[192,128]{1,0:T(8,128)(2,1)S(1)} %collective-permute-done.1.refs_0_, bf16[384,128]{1,0:T(8,128)(2,1)S(1)} %collective-permute-done.3.refs_1_, ...), custom_call_target="tpu_custom_call" | custom-call | flops 226492416 | bytes 884736 | tf_op jit(solution)/shard_map/pallas_call | solution.py:334
  21.0 0.1 collective-permute-start.6
  21.1 0.7 %shard_map.109 = (f32[48,2048]{1,0:T(8,128)S(1)}, bf16[48,2048]{1,0:T(8,128)(2,1)S(1)}, f32[48,2048]{1,0:T(8,128)S(1)}) custom-call(bf16[192,256]{1,0:T(8,128)(2,1)S(1)} %get-tuple-element.29.att_ref, bf16[256,2048]{1,0:T(8,128)(2,1)S(1)} %copy-done), custom_call_target="tpu_custom_call" | custom-call | flops 50331648 | bytes 196608 | tf_op jit(solution)/shard_map/pallas_call | solution.py:376
  21.8 0.5 %collective-permute-start.5 = (bf16[48,2048]{1,0:T(8,128)(2,1)S(1)}, bf16[48,2048]{1,0:T(8,128)(2,1)S(1)}, u32[]{:S(2)}, u32[]{:S(2)}) collective-permute-start(bf16[48,2048]{1,0:T(8,128)(2,1)S(1)} %get-tuple-element.31), channel_id=1, source_target_pairs={{0,1},{1,0},{2,3},{3,2},{4,5},{5,4},{6,7},{7,6},{8,9},{9,8},{10,11... | collective-permute-start | bytes 589832 | tf_op jit(solution)/shard_map/ppermute | solution.py:386
  22.3 0.2 collective-permute-done.6
  22.6 1.6 %collective-permute-start.7 = (bf16[48,2048]{1,0:T(8,128)(2,1)S(1)}, bf16[48,2048]{1,0:T(8,128)(2,1)S(1)}, u32[]{:S(2)}, u32[]{:S(2)}) collective-permute-start(bf16[48,2048]{1,0:T(8,128)(2,1)S(1)} %add_convert_fusion.1), channel_id=1, source_target_pairs={{0,2},{1,3},{2,0},{3,1},{4,6},{5,7},{6,4},{7,5},{8,10},{9,11},{10,... | collective-permute-start | bytes 589832 | tf_op jit(solution)/shard_map/ppermute | solution.py:386
  24.1 0.6 %log_add_fusion = f32[4,192]{1,0:T(4,128)} fusion(f32[4,192]{1,0:T(4,128)S(1)} %get-tuple-element.34, f32[4,192]{1,0:T(4,128)S(1)} %get-tuple-element.35), kind=kLoop, calls=%fused_computation.4 | loop fusion | flops 768 | bytes 9216 | tf_op jit(solution)/shard_map/add | solution.py:389
  24.7 0.0 collective-permute-done.5
  24.7 4.8 %collective-permute-done.7 = bf16[48,2048]{1,0:T(8,128)(2,1)S(1)} collective-permute-done((bf16[48,2048]{1,0:T(8,128)(2,1)S(1)}, bf16[48,2048]{1,0:T(8,128)(2,1)S(1)}, u32[]{:S(2)}, u32[]{:S(2)}) %collective-permute-start.7) | collective-permute-done | bytes 196640 | tf_op jit(solution)/shard_map/ppermute | solution.py:386
  29.6 0.8 %add_convert_fusion = bf16[48,2048]{1,0:T(8,128)(2,1)} fusion(bf16[48,2048]{1,0:T(8,128)(2,1)S(1)} %collective-permute-done.7, f32[48,2048]{1,0:T(8,128)S(1)} %get-tuple-element.30, bf16[48,2048]{1,0:T(8,128)(2,1)S(1)} %collective-permute-done.5), kind=kLoop, calls=%fused_computation | loop fusion | flops 491520 | bytes 983040 | tf_op jit(solution)/shard_map/convert_element_type | solution.py:389
  (3 shorter events, 0.1 us)
Async XLA Ops:
  0.6 0.7 %copy-start.4 = (f32[64]{0:T(128)S(1)}, f32[64]{0:T(128)}, u32[]{:S(2)}) copy-start(f32[64]{0:T(128)} %param.15) | copy-start | bytes 772
  1.3 15.8 %copy-start.1 = (bf16[192,2048]{1,0:T(8,128)(2,1)S(1)}, bf16[192,2048]{1,0:T(8,128)(2,1)}, u32[]{:S(2)}) copy-start(bf16[192,2048]{1,0:T(8,128)(2,1)} %tok_ref) | copy-start | bytes 2359300
  1.3 15.8 %copy-start.2 = (bf16[2048,256]{1,0:T(8,128)(2,1)S(1)}, bf16[2048,256]{1,0:T(8,128)(2,1)}, u32[]{:S(2)}) copy-start(bf16[2048,256]{1,0:T(8,128)(2,1)} %wq_ref) | copy-start | bytes 3145732
  3.3 13.8 %copy-start.3 = (f32[88,256]{1,0:T(8,128)S(1)}, f32[88,256]{1,0:T(8,128)}, u32[]{:S(2)}) copy-start(f32[88,256]{1,0:T(8,128)} %constant.5.clone.table_ref) | copy-start | bytes 270340
  3.3 5.1 %collective-permute-start.2 = (bf16[192,128]{1,0:T(8,128)(2,1)S(1)}, bf16[192,128]{1,0:T(8,128)(2,1)S(1)}, u32[]{:S(2)}, u32[]{:S(2)}) collective-permute-start(bf16[192,128]{1,0:T(8,128)(2,1)S(1)} %shard_map.104), channel_id=1, source_target_pairs={{0,4},{4,0},{8,12},{12,8},{16,20},{20,16},{24,28},{28,24},{1,5},{5... | collective-permute-start | bytes 147464 | tf_op jit(solution)/shard_map/ppermute | solution.py:349
  8.4 8.7 %copy-start.5 = (f32[64]{0:T(128)S(1)}, f32[64]{0:T(128)}, u32[]{:S(2)}) copy-start(f32[64]{0:T(128)} %param.14) | copy-start | bytes 772
  8.4 10.1 %collective-permute-start.4 = (bf16[384,128]{1,0:T(8,128)(2,1)S(1)}, bf16[384,128]{1,0:T(8,128)(2,1)S(1)}, u32[]{:S(2)}, u32[]{:S(2)}) collective-permute-start(bf16[384,128]{1,0:T(8,128)(2,1)S(1)} %constant_dynamic-update-slice_fusion.refs_0_), channel_id=1, source_target_pairs={{0,8},{4,12},{8,0},{12,4},{16,24},{20,28},{24,16},{28,20},{1,9},{5... | collective-permute-start | bytes 294920 | tf_op jit(solution)/shard_map/ppermute | solution.py:353
  10.6 5.0 %collective-permute-start = (bf16[192,128]{1,0:T(8,128)(2,1)S(1)}, bf16[192,128]{1,0:T(8,128)(2,1)S(1)}, u32[]{:S(2)}, u32[]{:S(2)}) collective-permute-start(bf16[192,128]{1,0:T(8,128)(2,1)S(1)} %shard_map.104), channel_id=1, source_target_pairs={{0,16},{4,20},{8,24},{12,28},{16,0},{20,4},{24,8},{28,12},{1,17},{... | collective-permute-start | bytes 147464 | tf_op jit(solution)/shard_map/ppermute | solution.py:350
  13.2 6.5 %collective-permute-start.3 = (bf16[384,128]{1,0:T(8,128)(2,1)S(1)}, bf16[384,128]{1,0:T(8,128)(2,1)S(1)}, u32[]{:S(2)}, u32[]{:S(2)}) collective-permute-start(bf16[384,128]{1,0:T(8,128)(2,1)S(1)} %constant_dynamic-update-slice_fusion.refs_0_), channel_id=1, source_target_pairs={{0,24},{4,28},{8,16},{12,20},{16,8},{20,12},{24,0},{28,4},{1,25},{... | collective-permute-start | bytes 294920 | tf_op jit(solution)/shard_map/ppermute | solution.py:352
  15.6 4.1 %collective-permute-start.1 = (bf16[192,128]{1,0:T(8,128)(2,1)S(1)}, bf16[192,128]{1,0:T(8,128)(2,1)S(1)}, u32[]{:S(2)}, u32[]{:S(2)}) collective-permute-start(bf16[192,128]{1,0:T(8,128)(2,1)S(1)} %collective-permute-done.refs_1_), channel_id=1, source_target_pairs={{0,4},{4,0},{8,12},{12,8},{16,20},{20,16},{24,28},{28,24},{1,5},{5... | collective-permute-start | bytes 147464 | tf_op jit(solution)/shard_map/ppermute | solution.py:354
  17.9 1.7 %copy-start = (bf16[256,2048]{1,0:T(8,128)(2,1)S(1)}, bf16[256,2048]{1,0:T(8,128)(2,1)}, u32[]{:S(2)}) copy-start(bf16[256,2048]{1,0:T(8,128)(2,1)} %wo_ref) | copy-start | bytes 3145732
  21.0 1.5 %collective-permute-start.6 = (bf16[48,2048]{1,0:T(8,128)(2,1)S(1)}, bf16[48,2048]{1,0:T(8,128)(2,1)S(1)}, u32[]{:S(2)}, u32[]{:S(2)}) collective-permute-start(bf16[48,2048]{1,0:T(8,128)(2,1)S(1)} %get-tuple-element.33), channel_id=1, source_target_pairs={{0,1},{1,0},{2,3},{3,2},{4,5},{5,4},{6,7},{7,6},{8,9},{9,8},{10,11... | collective-permute-start | bytes 589832 | tf_op jit(solution)/shard_map/ppermute | solution.py:386
  21.8 3.0 %collective-permute-start.5 = (bf16[48,2048]{1,0:T(8,128)(2,1)S(1)}, bf16[48,2048]{1,0:T(8,128)(2,1)S(1)}, u32[]{:S(2)}, u32[]{:S(2)}) collective-permute-start(bf16[48,2048]{1,0:T(8,128)(2,1)S(1)} %get-tuple-element.31), channel_id=1, source_target_pairs={{0,1},{1,0},{2,3},{3,2},{4,5},{5,4},{6,7},{7,6},{8,9},{9,8},{10,11... | collective-permute-start | bytes 589832 | tf_op jit(solution)/shard_map/ppermute | solution.py:386
  22.6 7.0 %collective-permute-start.7 = (bf16[48,2048]{1,0:T(8,128)(2,1)S(1)}, bf16[48,2048]{1,0:T(8,128)(2,1)S(1)}, u32[]{:S(2)}, u32[]{:S(2)}) collective-permute-start(bf16[48,2048]{1,0:T(8,128)(2,1)S(1)} %add_convert_fusion.1), channel_id=1, source_target_pairs={{0,2},{1,3},{2,0},{3,1},{4,6},{5,7},{6,4},{7,5},{8,10},{9,11},{10,... | collective-permute-start | bytes 589832 | tf_op jit(solution)/shard_map/ppermute | solution.py:386

commit v5 on v4

--- a/solution.py
+++ b/solution.py
@@ -14,7 +14,7 @@
 NORM_EPS = 1e-06
 LANES = 128
 LIMIT = 12 << 20
-SPAN = 768
+SPAN = 1024
 KV_LIMIT = 56480000
 
 
@@ -43,33 +43,19 @@
     return np.concatenate([table(GRID_W, ~by_row), rows]).astype(np.float32)
 
 
-def turn(values, row_start, table_ref, head_dim):
+def swap_matrix(head_dim):
     quarter = head_dim // 4
-    rows = values.shape[0]
+    source = lax.broadcasted_iota(jnp.int32, (LANES, LANES), 0)
+    target = lax.broadcasted_iota(jnp.int32, (LANES, LANES), 1)
+    step = jnp.where(target % (2 * quarter) < quarter, quarter, -quarter)
+    return jnp.where(source == target + step, 1.0, 0.0).astype(jnp.bfloat16)
+
+
+def swapped(row, head_dim):
+    quarter = head_dim // 4
     lane = lax.broadcasted_iota(jnp.int32, (1, LANES), 1)
-    ahead = pltpu.roll(values, LANES - quarter, 1)
-    behind = pltpu.roll(values, quarter, 1)
-    other = jnp.where(lane % (2 * quarter) < quarter, ahead, behind)
-    columns = table_ref[0:GRID_W, :]
-    out = []
-    for j in range(rows // GRID_W):
-        row = table_ref[pl.ds(GRID_W + row_start + j, 1), :]
-        both = columns + row
-        part = slice(j * GRID_W, (j + 1) * GRID_W)
-        out.append(values[part] * both[:, :LANES] + other[part] * both[:, LANES:])
-    return jnp.concatenate(out, axis=0)
-
-
-def normed(values, gain, head_dim):
-    lane = lax.broadcasted_iota(jnp.int32, (1, LANES), 1)
-    gain = jnp.concatenate([gain] * (LANES // head_dim), axis=1)
-    squares = values * values
-    scale = jnp.zeros_like(values)
-    for g in range(LANES // head_dim):
-        mine = lane // head_dim == g
-        mean = jnp.sum(jnp.where(mine, squares, 0.0), axis=1, keepdims=True) * (1.0 / head_dim)
-        scale = jnp.where(mine, lax.rsqrt(mean + NORM_EPS), scale)
-    return values * scale * gain
+    ahead, behind = pltpu.roll(row, LANES - quarter, 1), pltpu.roll(row, quarter, 1)
+    return jnp.where(lane % (2 * quarter) < quarter, ahead, behind)
 
 
 class Copies:
@@ -109,11 +95,7 @@
         )
         raw = more if raw is None else raw + more
     rounded = raw.astype(jnp.bfloat16)
-    quarter = head_dim // 4
-    source = lax.broadcasted_iota(jnp.int32, (LANES, LANES), 0)
-    target = lax.broadcasted_iota(jnp.int32, (LANES, LANES), 1)
-    step = jnp.where(target % (2 * quarter) < quarter, quarter, -quarter)
-    swap = jnp.where(source == target + step, 1.0, 0.0).astype(jnp.bfloat16)
+    swap = swap_matrix(head_dim)
     other = jnp.dot(rounded, swap, preferred_element_type=jnp.float32)
     raw = rounded.astype(jnp.float32)
     lane = lax.broadcasted_iota(jnp.int32, (1, LANES), 1)
@@ -121,8 +103,7 @@
     mean = jnp.sum(jnp.where(mine, raw * raw, 0.0), axis=1, keepdims=True) * (1.0 / head_dim)
     scale = lax.rsqrt(mean + NORM_EPS)
     gain = jnp.concatenate([gain_ref[...]] * (LANES // head_dim), axis=1)
-    ahead, behind = pltpu.roll(gain, LANES - quarter, 1), pltpu.roll(gain, quarter, 1)
-    other_gain = jnp.where(lane % (2 * quarter) < quarter, ahead, behind)
+    other_gain = swapped(gain, head_dim)
     row_start = lax.axis_index("sp") * (rows // GRID_W)
     copies.wait(3 * pieces, 3 * pieces + 1)
     columns = table_ref[0:GRID_W, :]
@@ -185,27 +166,44 @@
     return state
 
 
-def q_kernel(head_dim, tok_ref, wq_ref, gain_ref, table_ref, qt_ref):
+def q_kernel(head_dim, tok_ref, wq_ref, gain_ref, table_ref, *refs):
+    kv_refs = refs[:-6]
+    qt_ref, top_ref, total_ref, acc_ref, *spare = refs[-6:]
     rows = tok_ref.shape[0]
     heads = wq_ref.shape[1] // head_dim
     raw = jnp.dot(tok_ref[...], wq_ref[...], preferred_element_type=jnp.float32)
-    raw = raw.astype(jnp.bfloat16).astype(jnp.float32)
+    rounded = raw.astype(jnp.bfloat16)
     row_start = lax.axis_index("sp") * (rows // GRID_W)
     per = LANES // head_dim
+    lane = lax.broadcasted_iota(jnp.int32, (1, LANES), 1)
+    gain = jnp.concatenate([gain_ref[...]] * per, axis=1) * (head_dim ** -0.5)
+    other_gain = swapped(gain, head_dim)
+    swap = swap_matrix(head_dim)
+    turns = []
+    for j in range(rows // GRID_W):
+        both = table_ref[0:GRID_W, :] + table_ref[pl.ds(GRID_W + row_start + j, 1), :]
+        turns.append((gain * both[:, :LANES], other_gain * both[:, LANES:]))
     columns = []
     for p in range(heads // per):
-        x = raw[:, p * LANES : (p + 1) * LANES]
-        y = turn(normed(x, gain_ref[...], head_dim), row_start, table_ref, head_dim)
-        yt = (y * (head_dim ** -0.5)).T
+        part = rounded[:, p * LANES : (p + 1) * LANES]
+        other = jnp.dot(part, swap, preferred_element_type=jnp.float32)
+        x = part.astype(jnp.float32)
+        squares = x * x
+        scale = None
+        for g in range(per):
+            mine = lane // head_dim == g
+            mean = jnp.sum(jnp.where(mine, squares, 0.0), axis=1, keepdims=True) * (1.0 / head_dim)
+            own = lax.rsqrt(mean + NORM_EPS)
+            scale = own if scale is None else jnp.where(mine, own, scale)
+        y = []
+        for j, (cosine, sine) in enumerate(turns):
+            some = slice(j * GRID_W, (j + 1) * GRID_W)
+            y.append((x[some] * cosine + other[some] * sine) * scale[some])
+        yt = jnp.concatenate(y, axis=0).T
         columns += [yt[g * head_dim : (g + 1) * head_dim] for g in range(per)]
     qt = jnp.concatenate(columns, axis=1)
     qt = jnp.concatenate([qt, jnp.zeros((LANES - head_dim, qt.shape[1]), jnp.float32)], axis=0)
     qt_ref[...] = qt.astype(jnp.bfloat16)
-
-
-def first_kernel(head_dim, qt_ref, *refs):
-    kv_refs = refs[:-5]
-    top_ref, total_ref, acc_ref, *spare = refs[-5:]
     state = attend_all(qt_ref, kv_refs, head_dim, (None, None, None), *spare)
     top_ref[...], total_ref[...], acc_ref[...] = state
 
@@ -302,21 +300,15 @@
     def work(kvs):
         return sum(4 * size * x.shape[0] * LANES for x in kvs)
 
-    qt = call(
-        functools.partial(q_kernel, head_dim),
-        bf16((LANES, size)),
-        2 * rows * width * heads * head_dim,
-        [VMEM] * 4,
-    )(tokens, w_query, query_gain[None, :], table)
-
-    def first(qt, *kvs):
-        return call(
-            functools.partial(first_kernel, head_dim),
-            state_shape,
-            work(kvs),
-            [VMEM] * (1 + len(kvs)),
+    def first(*kvs):
+        qt, *state = call(
+            functools.partial(q_kernel, head_dim),
+            [bf16((LANES, size))] + state_shape,
+            2 * rows * width * heads * head_dim + work(kvs),
+            [VMEM] * (4 + len(kvs)),
             scratch_shapes=spare(kvs),
-        )(qt, *kvs)
+        )(tokens, w_query, query_gain[None, :], table, *kvs)
+        return qt, state
 
     def blocks(qt, state, *kvs):
         return call(
@@ -352,8 +344,7 @@
         middle = send(pair, perm=xor(n_sp, 6))
         beside = send(pair, perm=xor(n_sp, 2))
         relayed = send(far, perm=xor(n_sp, 1))
-        state = first(qt, pair)
-        state = blocks(qt, state, beside, far)
+        qt, state = first(pair, beside, far)
         attended, top, summed, sent = finish(qt, state, relayed, middle)
     else:
         held = kv
@@ -364,7 +355,7 @@
             radix = 2 if stride == 1 else min(4, n_sp // stride)
             got = [send(held, perm=xor(n_sp, d * stride)) for d in range(1, radix)]
             if state is None:
-                state = first(qt, *pending)
+                qt, state = first(*pending)
             else:
                 state = blocks(qt, state, *pending)
             pending = got

time: 30.5 us -> 30.5 us (level)
    pallas_call x3 -> x1, Pallas kernels: 2.38 us -> 2.29 us  [first(): call(functools.partial(q_kernel, head_dim), [bf16((LANES, size))] + state...]
where the time goes in v5:
time: 30.5 us; the launch traced here: 30.3 us
  starting transfers between devices  11.5 us (38%)
  waiting for transfers between devices  9.78 us (32%)
  Pallas kernels  6.28 us (21%)
  other arithmetic  1.4 us (5%)
  between operations  0.72 us (2%)
  local copies, waits for them, and re-layouts  0.69 us (2%)
    ppermute x3, waiting for transfers between devices, shards(): lax.ppermute(parts[d + bit].astype(jnp.bfloat16), 'tp', xor(n_tp, bit))  5.09 us
    ppermute x1, starting transfers between devices, shards(): near = send(kv, perm=xor(n_sp, 1))  3.07 us
    ppermute x1, starting transfers between devices, shards(): far = send(kv, perm=xor(n_sp, 4))  2.59 us
    ppermute x1, waiting for transfers between devices, shards(): far = send(kv, perm=xor(n_sp, 4))  2.39 us
    pallas_call x1, Pallas kernels, first(): call(functools.partial(q_kernel, head_dim), [bf16((LANES, size))] + state...  2.29 us
    ppermute x3, starting transfers between devices, shards(): lax.ppermute(parts[d + bit].astype(jnp.bfloat16), 'tp', xor(n_tp, bit))  2.16 us
    ppermute x1, starting transfers between devices, shards(): beside = send(pair, perm=xor(n_sp, 2))  2.14 us
    ppermute x1, waiting for transfers between devices, shards(): near = send(kv, perm=xor(n_sp, 1))  2.06 us
  transfers between devices with their start and end apart: 8, of which 5 were waited for; matrix products, arithmetic and copies ran while one was open for 2% of the time, Pallas kernels for 10%

profile of v5, /device:TPU:0, one launch (start us, length us, event | category | flops | bytes accessed | tf_op | source)
XLA Modules:
  0.0 30.3 jit_solution(14637467724261539126)
XLA Ops:
  0.6 0.0 copy-start.4
  0.6 0.6 %copy-done.4 = f32[64]{0:T(128)S(1)} copy-done((f32[64]{0:T(128)S(1)}, f32[64]{0:T(128)}, u32[]{:S(2)}) %copy-start.4) | copy-done | bytes 280
  1.3 0.0 copy-start.1
  1.3 0.0 copy-start.2
  1.3 2.0 %shard_map.104 = bf16[192,128]{1,0:T(8,128)(2,1)S(1)} custom-call(bf16[192,2048]{1,0:T(8,128)(2,1)} %tok_ref, bf16[64,2048]{1,0:T(8,128)(2,1)} %bitcast.6, bf16[64,2048]{1,0:T(8,128)(2,1)} %bitcast.7, f32[1,64]{1,0:T(1,128)S(1)} %bitcast.4, f32[88,2048]{1,0:T(8,128)} %constant.4.clone.table_hbm), custom_call_target="tpu_custom_call" | custom-call | flops 100663296 | bytes 393216 | tf_op jit(solution)/shard_map/pallas_call | solution.py:278
  3.3 0.0 copy-start.3
  3.3 3.1 %collective-permute-start = (bf16[192,128]{1,0:T(8,128)(2,1)S(1)}, bf16[192,128]{1,0:T(8,128)(2,1)S(1)}, u32[]{:S(2)}, u32[]{:S(2)}) collective-permute-start(bf16[192,128]{1,0:T(8,128)(2,1)S(1)} %shard_map.104), channel_id=1, source_target_pairs={{0,4},{4,0},{8,12},{12,8},{16,20},{20,16},{24,28},{28,24},{1,5},{5... | collective-permute-start | bytes 147464 | tf_op jit(solution)/shard_map/ppermute | solution.py:341
  6.4 2.1 %collective-permute-done = bf16[192,128]{1,0:T(8,128)(2,1)S(1)} collective-permute-done((bf16[192,128]{1,0:T(8,128)(2,1)S(1)}, bf16[192,128]{1,0:T(8,128)(2,1)S(1)}, u32[]{:S(2)}, u32[]{:S(2)}) %collective-permute-start) | collective-permute-done | bytes 49184 | tf_op jit(solution)/shard_map/ppermute | solution.py:341
  8.4 0.0 copy-start.5
  8.4 2.1 %collective-permute-start.1 = (bf16[384,128]{1,0:T(8,128)(2,1)S(1)}, bf16[384,128]{1,0:T(8,128)(2,1)S(1)}, u32[]{:S(2)}, u32[]{:S(2)}) collective-permute-start(bf16[384,128]{1,0:T(8,128)(2,1)S(1)} %constant_dynamic-update-slice_fusion.refs_0_), channel_id=1, source_target_pairs={{0,8},{4,12},{8,0},{12,4},{16,24},{20,28},{24,16},{28,20},{1,9},{5... | collective-permute-start | bytes 294920 | tf_op jit(solution)/shard_map/ppermute | solution.py:345
  10.6 2.6 %collective-permute-start.2 = (bf16[192,128]{1,0:T(8,128)(2,1)S(1)}, bf16[192,128]{1,0:T(8,128)(2,1)S(1)}, u32[]{:S(2)}, u32[]{:S(2)}) collective-permute-start(bf16[192,128]{1,0:T(8,128)(2,1)S(1)} %shard_map.104), channel_id=1, source_target_pairs={{0,16},{4,20},{8,24},{12,28},{16,0},{20,4},{24,8},{28,12},{1,17},{... | collective-permute-start | bytes 147464 | tf_op jit(solution)/shard_map/ppermute | solution.py:342
  13.2 0.0 collective-permute-start.4
  13.2 2.4 %collective-permute-done.2.refs_2_ = bf16[192,128]{1,0:T(8,128)(2,1)S(1)} collective-permute-done((bf16[192,128]{1,0:T(8,128)(2,1)S(1)}, bf16[192,128]{1,0:T(8,128)(2,1)S(1)}, u32[]{:S(2)}, u32[]{:S(2)}) %collective-permute-start.2) | collective-permute-done | bytes 49184 | tf_op jit(solution)/shard_map/ppermute | solution.py:342
  15.6 1.5 %collective-permute-start.3 = (bf16[192,128]{1,0:T(8,128)(2,1)S(1)}, bf16[192,128]{1,0:T(8,128)(2,1)S(1)}, u32[]{:S(2)}, u32[]{:S(2)}) collective-permute-start(bf16[192,128]{1,0:T(8,128)(2,1)S(1)} %collective-permute-done.2.refs_2_), channel_id=1, source_target_pairs={{0,4},{4,0},{8,12},{12,8},{16,20},{20,16},{24,28},{28,24},{1,5},{5... | collective-permute-start | bytes 147464 | tf_op jit(solution)/shard_map/ppermute | solution.py:346
  17.1 0.0 collective-permute-done.1.refs_1_
  17.1 0.0 copy-done.1
  17.1 0.0 copy-done.2
  17.1 0.0 copy-done.3
  17.1 0.0 copy-done.5
  17.1 0.0 copy-start
  17.1 2.3 %shard_map.105 = (bf16[128,768]{1,0:T(8,128)(2,1)S(1)}, f32[1,768]{1,0:T(1,128)S(1)}, f32[8,768]{1,0:T(8,128)S(1)}, f32[64,768]{1,0:T(8,128)S(1)}) custom-call(bf16[192,2048]{1,0:T(8,128)(2,1)S(1)} %copy-done.1, bf16[2048,256]{1,0:T(8,128)(2,1)S(1)} %copy-done.2, f32[1,64]{1,0:T(1,128)S(1)} %bitcast.5, f32[88,256]{1,0:T(8,128)S(1)} %copy-done.3, ...), custom_call_target="tpu_custom_call" | custom-call | flops 578813952 | bytes 2260992 | tf_op jit(solution)/shard_map/pallas_call | solution.py:304
  19.4 0.2 collective-permute-done.3.refs_0_
  19.7 0.0 collective-permute-done.4.refs_1_
  19.7 0.0 copy-done
  19.7 1.4 %shard_map.106 = (bf16[192,256]{1,0:T(8,128)(2,1)S(1)}, f32[4,192]{1,0:T(4,128)S(1)}, f32[4,192]{1,0:T(4,128)S(1)}, bf16[48,2048]{1,0:T(8,128)(2,1)S(1)}) custom-call(bf16[128,768]{1,0:T(8,128)(2,1)S(1)} %get-tuple-element.20.qt_ref, bf16[192,128]{1,0:T(8,128)(2,1)S(1)} %collective-permute-done.3.refs_0_, ...), custom_call_target="tpu_custom_call" | custom-call | flops 226492416 | bytes 884736 | tf_op jit(solution)/shard_map/pallas_call | solution.py:326
  21.0 0.1 collective-permute-start.6
  21.1 0.7 %shard_map.107 = (f32[48,2048]{1,0:T(8,128)S(1)}, bf16[48,2048]{1,0:T(8,128)(2,1)S(1)}, f32[48,2048]{1,0:T(8,128)S(1)}) custom-call(bf16[192,256]{1,0:T(8,128)(2,1)S(1)} %get-tuple-element.25.att_ref, bf16[256,2048]{1,0:T(8,128)(2,1)S(1)} %copy-done), custom_call_target="tpu_custom_call" | custom-call | flops 50331648 | bytes 196608 | tf_op jit(solution)/shard_map/pallas_call | solution.py:367
  21.8 0.5 %collective-permute-start.5 = (bf16[48,2048]{1,0:T(8,128)(2,1)S(1)}, bf16[48,2048]{1,0:T(8,128)(2,1)S(1)}, u32[]{:S(2)}, u32[]{:S(2)}) collective-permute-start(bf16[48,2048]{1,0:T(8,128)(2,1)S(1)} %get-tuple-element.27), channel_id=1, source_target_pairs={{0,1},{1,0},{2,3},{3,2},{4,5},{5,4},{6,7},{7,6},{8,9},{9,8},{10,11... | collective-permute-start | bytes 589832 | tf_op jit(solution)/shard_map/ppermute | solution.py:377
  22.3 0.2 collective-permute-done.6
  22.5 0.1 add_convert_fusion.1
  22.6 1.6 %collective-permute-start.7 = (bf16[48,2048]{1,0:T(8,128)(2,1)S(1)}, bf16[48,2048]{1,0:T(8,128)(2,1)S(1)}, u32[]{:S(2)}, u32[]{:S(2)}) collective-permute-start(bf16[48,2048]{1,0:T(8,128)(2,1)S(1)} %add_convert_fusion.1), channel_id=1, source_target_pairs={{0,2},{1,3},{2,0},{3,1},{4,6},{5,7},{6,4},{7,5},{8,10},{9,11},{10,... | collective-permute-start | bytes 589832 | tf_op jit(solution)/shard_map/ppermute | solution.py:377
  24.1 0.6 %log_add_fusion = f32[4,192]{1,0:T(4,128)} fusion(f32[4,192]{1,0:T(4,128)S(1)} %get-tuple-element.30, f32[4,192]{1,0:T(4,128)S(1)} %get-tuple-element.31), kind=kLoop, calls=%fused_computation.4 | loop fusion | flops 768 | bytes 9216 | tf_op jit(solution)/shard_map/add | solution.py:380
  24.7 0.0 collective-permute-done.5
  24.8 4.8 %collective-permute-done.7 = bf16[48,2048]{1,0:T(8,128)(2,1)S(1)} collective-permute-done((bf16[48,2048]{1,0:T(8,128)(2,1)S(1)}, bf16[48,2048]{1,0:T(8,128)(2,1)S(1)}, u32[]{:S(2)}, u32[]{:S(2)}) %collective-permute-start.7) | collective-permute-done | bytes 196640 | tf_op jit(solution)/shard_map/ppermute | solution.py:377
  29.6 0.7 %add_convert_fusion = bf16[48,2048]{1,0:T(8,128)(2,1)} fusion(bf16[48,2048]{1,0:T(8,128)(2,1)S(1)} %collective-permute-done.7, f32[48,2048]{1,0:T(8,128)S(1)} %get-tuple-element.26, bf16[48,2048]{1,0:T(8,128)(2,1)S(1)} %collective-permute-done.5), kind=kLoop, calls=%fused_computation | loop fusion | flops 491520 | bytes 983040 | tf_op jit(solution)/shard_map/convert_element_type | solution.py:380
  (2 shorter events, 0.0 us)
Async XLA Ops:
  0.6 0.7 %copy-start.4 = (f32[64]{0:T(128)S(1)}, f32[64]{0:T(128)}, u32[]{:S(2)}) copy-start(f32[64]{0:T(128)} %param.15) | copy-start | bytes 772
  1.3 15.8 %copy-start.1 = (bf16[192,2048]{1,0:T(8,128)(2,1)S(1)}, bf16[192,2048]{1,0:T(8,128)(2,1)}, u32[]{:S(2)}) copy-start(bf16[192,2048]{1,0:T(8,128)(2,1)} %tok_ref) | copy-start | bytes 2359300
  1.3 15.8 %copy-start.2 = (bf16[2048,256]{1,0:T(8,128)(2,1)S(1)}, bf16[2048,256]{1,0:T(8,128)(2,1)}, u32[]{:S(2)}) copy-start(bf16[2048,256]{1,0:T(8,128)(2,1)} %wq_ref) | copy-start | bytes 3145732
  3.3 13.8 %copy-start.3 = (f32[88,256]{1,0:T(8,128)S(1)}, f32[88,256]{1,0:T(8,128)}, u32[]{:S(2)}) copy-start(f32[88,256]{1,0:T(8,128)} %constant.5.clone.table_ref) | copy-start | bytes 270340
  3.3 5.1 %collective-permute-start = (bf16[192,128]{1,0:T(8,128)(2,1)S(1)}, bf16[192,128]{1,0:T(8,128)(2,1)S(1)}, u32[]{:S(2)}, u32[]{:S(2)}) collective-permute-start(bf16[192,128]{1,0:T(8,128)(2,1)S(1)} %shard_map.104), channel_id=1, source_target_pairs={{0,4},{4,0},{8,12},{12,8},{16,20},{20,16},{24,28},{28,24},{1,5},{5... | collective-permute-start | bytes 147464 | tf_op jit(solution)/shard_map/ppermute | solution.py:341
  8.4 8.7 %copy-start.5 = (f32[64]{0:T(128)S(1)}, f32[64]{0:T(128)}, u32[]{:S(2)}) copy-start(f32[64]{0:T(128)} %param.14) | copy-start | bytes 772
  8.4 8.7 %collective-permute-start.1 = (bf16[384,128]{1,0:T(8,128)(2,1)S(1)}, bf16[384,128]{1,0:T(8,128)(2,1)S(1)}, u32[]{:S(2)}, u32[]{:S(2)}) collective-permute-start(bf16[384,128]{1,0:T(8,128)(2,1)S(1)} %constant_dynamic-update-slice_fusion.refs_0_), channel_id=1, source_target_pairs={{0,8},{4,12},{8,0},{12,4},{16,24},{20,28},{24,16},{28,20},{1,9},{5... | collective-permute-start | bytes 294920 | tf_op jit(solution)/shard_map/ppermute | solution.py:345
  10.6 5.0 %collective-permute-start.2 = (bf16[192,128]{1,0:T(8,128)(2,1)S(1)}, bf16[192,128]{1,0:T(8,128)(2,1)S(1)}, u32[]{:S(2)}, u32[]{:S(2)}) collective-permute-start(bf16[192,128]{1,0:T(8,128)(2,1)S(1)} %shard_map.104), channel_id=1, source_target_pairs={{0,16},{4,20},{8,24},{12,28},{16,0},{20,4},{24,8},{28,12},{1,17},{... | collective-permute-start | bytes 147464 | tf_op jit(solution)/shard_map/ppermute | solution.py:342
  13.2 6.5 %collective-permute-start.4 = (bf16[384,128]{1,0:T(8,128)(2,1)S(1)}, bf16[384,128]{1,0:T(8,128)(2,1)S(1)}, u32[]{:S(2)}, u32[]{:S(2)}) collective-permute-start(bf16[384,128]{1,0:T(8,128)(2,1)S(1)} %constant_dynamic-update-slice_fusion.refs_0_), channel_id=1, source_target_pairs={{0,24},{4,28},{8,16},{12,20},{16,8},{20,12},{24,0},{28,4},{1,25},{... | collective-permute-start | bytes 294920 | tf_op jit(solution)/shard_map/ppermute | solution.py:344
  15.6 4.1 %collective-permute-start.3 = (bf16[192,128]{1,0:T(8,128)(2,1)S(1)}, bf16[192,128]{1,0:T(8,128)(2,1)S(1)}, u32[]{:S(2)}, u32[]{:S(2)}) collective-permute-start(bf16[192,128]{1,0:T(8,128)(2,1)S(1)} %collective-permute-done.2.refs_2_), channel_id=1, source_target_pairs={{0,4},{4,0},{8,12},{12,8},{16,20},{20,16},{24,28},{28,24},{1,5},{5... | collective-permute-start | bytes 147464 | tf_op jit(solution)/shard_map/ppermute | solution.py:346
  17.1 2.5 %copy-start = (bf16[256,2048]{1,0:T(8,128)(2,1)S(1)}, bf16[256,2048]{1,0:T(8,128)(2,1)}, u32[]{:S(2)}) copy-start(bf16[256,2048]{1,0:T(8,128)(2,1)} %wo_ref) | copy-start | bytes 3145732
  21.0 1.5 %collective-permute-start.6 = (bf16[48,2048]{1,0:T(8,128)(2,1)S(1)}, bf16[48,2048]{1,0:T(8,128)(2,1)S(1)}, u32[]{:S(2)}, u32[]{:S(2)}) collective-permute-start(bf16[48,2048]{1,0:T(8,128)(2,1)S(1)} %get-tuple-element.29), channel_id=1, source_target_pairs={{0,1},{1,0},{2,3},{3,2},{4,5},{5,4},{6,7},{7,6},{8,9},{9,8},{10,11... | collective-permute-start | bytes 589832 | tf_op jit(solution)/shard_map/ppermute | solution.py:377
  21.8 3.0 %collective-permute-start.5 = (bf16[48,2048]{1,0:T(8,128)(2,1)S(1)}, bf16[48,2048]{1,0:T(8,128)(2,1)S(1)}, u32[]{:S(2)}, u32[]{:S(2)}) collective-permute-start(bf16[48,2048]{1,0:T(8,128)(2,1)S(1)} %get-tuple-element.27), channel_id=1, source_target_pairs={{0,1},{1,0},{2,3},{3,2},{4,5},{5,4},{6,7},{7,6},{8,9},{9,8},{10,11... | collective-permute-start | bytes 589832 | tf_op jit(solution)/shard_map/ppermute | solution.py:377
  22.6 7.0 %collective-permute-start.7 = (bf16[48,2048]{1,0:T(8,128)(2,1)S(1)}, bf16[48,2048]{1,0:T(8,128)(2,1)S(1)}, u32[]{:S(2)}, u32[]{:S(2)}) collective-permute-start(bf16[48,2048]{1,0:T(8,128)(2,1)S(1)} %add_convert_fusion.1), channel_id=1, source_target_pairs={{0,2},{1,3},{2,0},{3,1},{4,6},{5,7},{6,4},{7,5},{8,10},{9,11},{10,... | collective-permute-start | bytes 589832 | tf_op jit(solution)/shard_map/ppermute | solution.py:377

commit v6 on v5

--- a/solution.py
+++ b/solution.py
@@ -74,43 +74,36 @@
 
 
 def kv_kernel(
-    head_dim, pieces, tok_hbm, wk_hbm, wv_hbm, gain_ref, table_hbm,
+    head_dim, tok_hbm, wk_hbm, wv_hbm, gain_ref, table_hbm,
     out_ref, tok_ref, both_ref, table_ref, sems,
 ):
-    rows, width = tok_ref.shape
-    step = width // pieces
+    rows, _ = tok_ref.shape
     copies = Copies(sems)
-    for i in range(pieces):
-        part = pl.ds(i * step, step)
-        copies.start(tok_hbm.at[:, part], tok_ref.at[:, part])
-        copies.start(wk_hbm.at[:, part], both_ref.at[pl.ds(0, head_dim), part])
-        copies.start(wv_hbm.at[:, part], both_ref.at[pl.ds(head_dim, head_dim), part])
     copies.start(table_hbm.at[:, pl.ds(0, 2 * LANES)], table_ref)
-    raw = None
-    for i in range(pieces):
-        copies.wait(3 * i, 3 * i + 3)
-        part = slice(i * step, (i + 1) * step)
-        more = lax.dot_general(
-            tok_ref[:, part], both_ref[:, part], NT, preferred_element_type=jnp.float32
-        )
-        raw = more if raw is None else raw + more
-    rounded = raw.astype(jnp.bfloat16)
+    copies.start(wk_hbm, both_ref.at[pl.ds(0, head_dim)])
+    copies.start(wv_hbm, both_ref.at[pl.ds(head_dim, head_dim)])
+    copies.start(tok_hbm, tok_ref)
     swap = swap_matrix(head_dim)
-    other = jnp.dot(rounded, swap, preferred_element_type=jnp.float32)
-    raw = rounded.astype(jnp.float32)
     lane = lax.broadcasted_iota(jnp.int32, (1, LANES), 1)
     mine = lane < head_dim
-    mean = jnp.sum(jnp.where(mine, raw * raw, 0.0), axis=1, keepdims=True) * (1.0 / head_dim)
-    scale = lax.rsqrt(mean + NORM_EPS)
     gain = jnp.concatenate([gain_ref[...]] * (LANES // head_dim), axis=1)
     other_gain = swapped(gain, head_dim)
     row_start = lax.axis_index("sp") * (rows // GRID_W)
-    copies.wait(3 * pieces, 3 * pieces + 1)
-    columns = table_ref[0:GRID_W, :]
+    copies.wait(0, 1)
+    turns = []
     for j in range(rows // GRID_W):
+        both = table_ref[0:GRID_W, :] + table_ref[pl.ds(GRID_W + row_start + j, 1), :]
+        turns.append((gain * both[:, :LANES], other_gain * both[:, LANES:]))
+    copies.wait(1, 4)
+    raw = lax.dot_general(tok_ref[...], both_ref[...], NT, preferred_element_type=jnp.float32)
+    rounded = raw.astype(jnp.bfloat16)
+    other = jnp.dot(rounded, swap, preferred_element_type=jnp.float32)
+    raw = rounded.astype(jnp.float32)
+    mean = jnp.sum(jnp.where(mine, raw * raw, 0.0), axis=1, keepdims=True) * (1.0 / head_dim)
+    scale = lax.rsqrt(mean + NORM_EPS)
+    for j, (cosine, sine) in enumerate(turns):
         part = slice(j * GRID_W, (j + 1) * GRID_W)
-        both = columns + table_ref[pl.ds(GRID_W + row_start + j, 1), :]
-        keys = raw[part] * (gain * both[:, :LANES]) + other[part] * (other_gain * both[:, LANES:])
+        keys = raw[part] * cosine + other[part] * sine
         out = jnp.where(mine, keys * scale[part], raw[part])
         out_ref[part, :] = out.astype(jnp.bfloat16)
 
@@ -276,7 +269,7 @@
 
     scratch = [pltpu.VMEM((1, head_dim), jnp.float32), pltpu.VMEM((table.shape[0], 2 * LANES), jnp.float32)]
     kv = call(
-        functools.partial(kv_kernel, head_dim, pieces),
+        functools.partial(kv_kernel, head_dim),
         bf16((rows, LANES)),
         2 * rows * width * LANES,
         [HBM] * 3 + [VMEM, HBM],

time: 30.5 us -> 30.5 us (level)
  no operation moved by 1% of the time
where the time goes in v6:
time: 30.5 us; the launch traced here: 30.4 us
  starting transfers between devices  11.5 us (38%)
  waiting for transfers between devices  9.77 us (32%)
  Pallas kernels  6.33 us (21%)
  other arithmetic  1.4 us (5%)
  between operations  0.72 us (2%)
  local copies, waits for them, and re-layouts  0.69 us (2%)
    ppermute x3, waiting for transfers between devices, shards(): lax.ppermute(parts[d + bit].astype(jnp.bfloat16), 'tp', xor(n_tp, bit))  5.08 us
    ppermute x1, starting transfers between devices, shards(): near = send(kv, perm=xor(n_sp, 1))  3.06 us
    ppermute x1, starting transfers between devices, shards(): far = send(kv, perm=xor(n_sp, 4))  2.6 us
    ppermute x1, waiting for transfers between devices, shards(): far = send(kv, perm=xor(n_sp, 4))  2.39 us
    pallas_call x1, Pallas kernels, first(): call(functools.partial(q_kernel, head_dim), [bf16((LANES, size))] + state...  2.29 us
    ppermute x3, starting transfers between devices, shards(): lax.ppermute(parts[d + bit].astype(jnp.bfloat16), 'tp', xor(n_tp, bit))  2.17 us
    ppermute x1, starting transfers between devices, shards(): beside = send(pair, perm=xor(n_sp, 2))  2.14 us
    ppermute x1, waiting for transfers between devices, shards(): near = send(kv, perm=xor(n_sp, 1))  2.06 us
  transfers between devices with their start and end apart: 8, of which 5 were waited for; matrix products, arithmetic and copies ran while one was open for 2% of the time, Pallas kernels for 10%

profile of v6, /device:TPU:0, one launch (start us, length us, event | category | flops | bytes accessed | tf_op | source)
XLA Modules:
  0.0 30.4 jit_solution(82440113003406649)
XLA Ops:
  0.6 0.0 copy-start.4
  0.6 0.6 %copy-done.4 = f32[64]{0:T(128)S(1)} copy-done((f32[64]{0:T(128)S(1)}, f32[64]{0:T(128)}, u32[]{:S(2)}) %copy-start.4) | copy-done | bytes 280
  1.3 0.0 copy-start.1
  1.3 0.0 copy-start.2
  1.3 2.0 %shard_map.104 = bf16[192,128]{1,0:T(8,128)(2,1)S(1)} custom-call(bf16[192,2048]{1,0:T(8,128)(2,1)} %tok_ref, bf16[64,2048]{1,0:T(8,128)(2,1)} %bitcast.6, bf16[64,2048]{1,0:T(8,128)(2,1)} %bitcast.7, f32[1,64]{1,0:T(1,128)S(1)} %bitcast.4, f32[88,2048]{1,0:T(8,128)} %constant.4.clone.table_hbm), custom_call_target="tpu_custom_call" | custom-call | flops 100663296 | bytes 393216 | tf_op jit(solution)/shard_map/pallas_call | solution.py:271
  3.3 0.0 copy-start.3
  3.3 3.1 %collective-permute-start = (bf16[192,128]{1,0:T(8,128)(2,1)S(1)}, bf16[192,128]{1,0:T(8,128)(2,1)S(1)}, u32[]{:S(2)}, u32[]{:S(2)}) collective-permute-start(bf16[192,128]{1,0:T(8,128)(2,1)S(1)} %shard_map.104), channel_id=1, source_target_pairs={{0,4},{4,0},{8,12},{12,8},{16,20},{20,16},{24,28},{28,24},{1,5},{5... | collective-permute-start | bytes 147464 | tf_op jit(solution)/shard_map/ppermute | solution.py:334
  6.4 2.1 %collective-permute-done = bf16[192,128]{1,0:T(8,128)(2,1)S(1)} collective-permute-done((bf16[192,128]{1,0:T(8,128)(2,1)S(1)}, bf16[192,128]{1,0:T(8,128)(2,1)S(1)}, u32[]{:S(2)}, u32[]{:S(2)}) %collective-permute-start) | collective-permute-done | bytes 49184 | tf_op jit(solution)/shard_map/ppermute | solution.py:334
  8.5 0.0 copy-start.5
  8.5 2.1 %collective-permute-start.1 = (bf16[384,128]{1,0:T(8,128)(2,1)S(1)}, bf16[384,128]{1,0:T(8,128)(2,1)S(1)}, u32[]{:S(2)}, u32[]{:S(2)}) collective-permute-start(bf16[384,128]{1,0:T(8,128)(2,1)S(1)} %constant_dynamic-update-slice_fusion.refs_0_), channel_id=1, source_target_pairs={{0,8},{4,12},{8,0},{12,4},{16,24},{20,28},{24,16},{28,20},{1,9},{5... | collective-permute-start | bytes 294920 | tf_op jit(solution)/shard_map/ppermute | solution.py:338
  10.6 2.6 %collective-permute-start.2 = (bf16[192,128]{1,0:T(8,128)(2,1)S(1)}, bf16[192,128]{1,0:T(8,128)(2,1)S(1)}, u32[]{:S(2)}, u32[]{:S(2)}) collective-permute-start(bf16[192,128]{1,0:T(8,128)(2,1)S(1)} %shard_map.104), channel_id=1, source_target_pairs={{0,16},{4,20},{8,24},{12,28},{16,0},{20,4},{24,8},{28,12},{1,17},{... | collective-permute-start | bytes 147464 | tf_op jit(solution)/shard_map/ppermute | solution.py:335
  13.2 0.0 collective-permute-start.4
  13.2 2.4 %collective-permute-done.2.refs_2_ = bf16[192,128]{1,0:T(8,128)(2,1)S(1)} collective-permute-done((bf16[192,128]{1,0:T(8,128)(2,1)S(1)}, bf16[192,128]{1,0:T(8,128)(2,1)S(1)}, u32[]{:S(2)}, u32[]{:S(2)}) %collective-permute-start.2) | collective-permute-done | bytes 49184 | tf_op jit(solution)/shard_map/ppermute | solution.py:335
  15.6 1.5 %collective-permute-start.3 = (bf16[192,128]{1,0:T(8,128)(2,1)S(1)}, bf16[192,128]{1,0:T(8,128)(2,1)S(1)}, u32[]{:S(2)}, u32[]{:S(2)}) collective-permute-start(bf16[192,128]{1,0:T(8,128)(2,1)S(1)} %collective-permute-done.2.refs_2_), channel_id=1, source_target_pairs={{0,4},{4,0},{8,12},{12,8},{16,20},{20,16},{24,28},{28,24},{1,5},{5... | collective-permute-start | bytes 147464 | tf_op jit(solution)/shard_map/ppermute | solution.py:339
  17.1 0.0 collective-permute-done.1.refs_1_
  17.1 0.0 copy-done.1
  17.1 0.0 copy-done.2
  17.1 0.0 copy-done.3
  17.2 0.0 copy-done.5
  17.2 0.0 copy-start
  17.2 2.3 %shard_map.105 = (bf16[128,768]{1,0:T(8,128)(2,1)S(1)}, f32[1,768]{1,0:T(1,128)S(1)}, f32[8,768]{1,0:T(8,128)S(1)}, f32[64,768]{1,0:T(8,128)S(1)}) custom-call(bf16[192,2048]{1,0:T(8,128)(2,1)S(1)} %copy-done.1, bf16[2048,256]{1,0:T(8,128)(2,1)S(1)} %copy-done.2, f32[1,64]{1,0:T(1,128)S(1)} %bitcast.5, f32[88,256]{1,0:T(8,128)S(1)} %copy-done.3, ...), custom_call_target="tpu_custom_call" | custom-call | flops 578813952 | bytes 2260992 | tf_op jit(solution)/shard_map/pallas_call | solution.py:297
  19.5 0.2 collective-permute-done.3.refs_0_
  19.7 0.0 collective-permute-done.4.refs_1_
  19.7 0.0 copy-done
  19.7 1.4 %shard_map.106 = (bf16[192,256]{1,0:T(8,128)(2,1)S(1)}, f32[4,192]{1,0:T(4,128)S(1)}, f32[4,192]{1,0:T(4,128)S(1)}, bf16[48,2048]{1,0:T(8,128)(2,1)S(1)}) custom-call(bf16[128,768]{1,0:T(8,128)(2,1)S(1)} %get-tuple-element.20.qt_ref, bf16[192,128]{1,0:T(8,128)(2,1)S(1)} %collective-permute-done.3.refs_0_, ...), custom_call_target="tpu_custom_call" | custom-call | flops 226492416 | bytes 884736 | tf_op jit(solution)/shard_map/pallas_call | solution.py:319
  21.1 0.1 collective-permute-start.6
  21.1 0.7 %shard_map.107 = (f32[48,2048]{1,0:T(8,128)S(1)}, bf16[48,2048]{1,0:T(8,128)(2,1)S(1)}, f32[48,2048]{1,0:T(8,128)S(1)}) custom-call(bf16[192,256]{1,0:T(8,128)(2,1)S(1)} %get-tuple-element.25.att_ref, bf16[256,2048]{1,0:T(8,128)(2,1)S(1)} %copy-done), custom_call_target="tpu_custom_call" | custom-call | flops 50331648 | bytes 196608 | tf_op jit(solution)/shard_map/pallas_call | solution.py:360
  21.8 0.5 %collective-permute-start.5 = (bf16[48,2048]{1,0:T(8,128)(2,1)S(1)}, bf16[48,2048]{1,0:T(8,128)(2,1)S(1)}, u32[]{:S(2)}, u32[]{:S(2)}) collective-permute-start(bf16[48,2048]{1,0:T(8,128)(2,1)S(1)} %get-tuple-element.27), channel_id=1, source_target_pairs={{0,1},{1,0},{2,3},{3,2},{4,5},{5,4},{6,7},{7,6},{8,9},{9,8},{10,11... | collective-permute-start | bytes 589832 | tf_op jit(solution)/shard_map/ppermute | solution.py:370
  22.3 0.2 collective-permute-done.6
  22.6 0.1 add_convert_fusion.1
  22.6 1.6 %collective-permute-start.7 = (bf16[48,2048]{1,0:T(8,128)(2,1)S(1)}, bf16[48,2048]{1,0:T(8,128)(2,1)S(1)}, u32[]{:S(2)}, u32[]{:S(2)}) collective-permute-start(bf16[48,2048]{1,0:T(8,128)(2,1)S(1)} %add_convert_fusion.1), channel_id=1, source_target_pairs={{0,2},{1,3},{2,0},{3,1},{4,6},{5,7},{6,4},{7,5},{8,10},{9,11},{10,... | collective-permute-start | bytes 589832 | tf_op jit(solution)/shard_map/ppermute | solution.py:370
  24.2 0.6 %log_add_fusion = f32[4,192]{1,0:T(4,128)} fusion(f32[4,192]{1,0:T(4,128)S(1)} %get-tuple-element.30, f32[4,192]{1,0:T(4,128)S(1)} %get-tuple-element.31), kind=kLoop, calls=%fused_computation.4 | loop fusion | flops 768 | bytes 9216 | tf_op jit(solution)/shard_map/add | solution.py:373
  24.8 0.0 collective-permute-done.5
  24.8 4.8 %collective-permute-done.7 = bf16[48,2048]{1,0:T(8,128)(2,1)S(1)} collective-permute-done((bf16[48,2048]{1,0:T(8,128)(2,1)S(1)}, bf16[48,2048]{1,0:T(8,128)(2,1)S(1)}, u32[]{:S(2)}, u32[]{:S(2)}) %collective-permute-start.7) | collective-permute-done | bytes 196640 | tf_op jit(solution)/shard_map/ppermute | solution.py:370
  29.6 0.7 %add_convert_fusion = bf16[48,2048]{1,0:T(8,128)(2,1)} fusion(bf16[48,2048]{1,0:T(8,128)(2,1)S(1)} %collective-permute-done.7, f32[48,2048]{1,0:T(8,128)S(1)} %get-tuple-element.26, bf16[48,2048]{1,0:T(8,128)(2,1)S(1)} %collective-permute-done.5), kind=kLoop, calls=%fused_computation | loop fusion | flops 491520 | bytes 983040 | tf_op jit(solution)/shard_map/convert_element_type | solution.py:373
  (2 shorter events, 0.0 us)
Async XLA Ops:
  0.6 0.7 %copy-start.4 = (f32[64]{0:T(128)S(1)}, f32[64]{0:T(128)}, u32[]{:S(2)}) copy-start(f32[64]{0:T(128)} %param.15) | copy-start | bytes 772
  1.3 15.9 %copy-start.1 = (bf16[192,2048]{1,0:T(8,128)(2,1)S(1)}, bf16[192,2048]{1,0:T(8,128)(2,1)}, u32[]{:S(2)}) copy-start(bf16[192,2048]{1,0:T(8,128)(2,1)} %tok_ref) | copy-start | bytes 2359300
  1.3 15.9 %copy-start.2 = (bf16[2048,256]{1,0:T(8,128)(2,1)S(1)}, bf16[2048,256]{1,0:T(8,128)(2,1)}, u32[]{:S(2)}) copy-start(bf16[2048,256]{1,0:T(8,128)(2,1)} %wq_ref) | copy-start | bytes 3145732
  3.3 13.8 %copy-start.3 = (f32[88,256]{1,0:T(8,128)S(1)}, f32[88,256]{1,0:T(8,128)}, u32[]{:S(2)}) copy-start(f32[88,256]{1,0:T(8,128)} %constant.5.clone.table_ref) | copy-start | bytes 270340
  3.3 5.1 %collective-permute-start = (bf16[192,128]{1,0:T(8,128)(2,1)S(1)}, bf16[192,128]{1,0:T(8,128)(2,1)S(1)}, u32[]{:S(2)}, u32[]{:S(2)}) collective-permute-start(bf16[192,128]{1,0:T(8,128)(2,1)S(1)} %shard_map.104), channel_id=1, source_target_pairs={{0,4},{4,0},{8,12},{12,8},{16,20},{20,16},{24,28},{28,24},{1,5},{5... | collective-permute-start | bytes 147464 | tf_op jit(solution)/shard_map/ppermute | solution.py:334
  8.5 8.7 %copy-start.5 = (f32[64]{0:T(128)S(1)}, f32[64]{0:T(128)}, u32[]{:S(2)}) copy-start(f32[64]{0:T(128)} %param.14) | copy-start | bytes 772
  8.5 8.6 %collective-permute-start.1 = (bf16[384,128]{1,0:T(8,128)(2,1)S(1)}, bf16[384,128]{1,0:T(8,128)(2,1)S(1)}, u32[]{:S(2)}, u32[]{:S(2)}) collective-permute-start(bf16[384,128]{1,0:T(8,128)(2,1)S(1)} %constant_dynamic-update-slice_fusion.refs_0_), channel_id=1, source_target_pairs={{0,8},{4,12},{8,0},{12,4},{16,24},{20,28},{24,16},{28,20},{1,9},{5... | collective-permute-start | bytes 294920 | tf_op jit(solution)/shard_map/ppermute | solution.py:338
  10.6 5.0 %collective-permute-start.2 = (bf16[192,128]{1,0:T(8,128)(2,1)S(1)}, bf16[192,128]{1,0:T(8,128)(2,1)S(1)}, u32[]{:S(2)}, u32[]{:S(2)}) collective-permute-start(bf16[192,128]{1,0:T(8,128)(2,1)S(1)} %shard_map.104), channel_id=1, source_target_pairs={{0,16},{4,20},{8,24},{12,28},{16,0},{20,4},{24,8},{28,12},{1,17},{... | collective-permute-start | bytes 147464 | tf_op jit(solution)/shard_map/ppermute | solution.py:335
  13.2 6.5 %collective-permute-start.4 = (bf16[384,128]{1,0:T(8,128)(2,1)S(1)}, bf16[384,128]{1,0:T(8,128)(2,1)S(1)}, u32[]{:S(2)}, u32[]{:S(2)}) collective-permute-start(bf16[384,128]{1,0:T(8,128)(2,1)S(1)} %constant_dynamic-update-slice_fusion.refs_0_), channel_id=1, source_target_pairs={{0,24},{4,28},{8,16},{12,20},{16,8},{20,12},{24,0},{28,4},{1,25},{... | collective-permute-start | bytes 294920 | tf_op jit(solution)/shard_map/ppermute | solution.py:337
  15.6 4.1 %collective-permute-start.3 = (bf16[192,128]{1,0:T(8,128)(2,1)S(1)}, bf16[192,128]{1,0:T(8,128)(2,1)S(1)}, u32[]{:S(2)}, u32[]{:S(2)}) collective-permute-start(bf16[192,128]{1,0:T(8,128)(2,1)S(1)} %collective-permute-done.2.refs_2_), channel_id=1, source_target_pairs={{0,4},{4,0},{8,12},{12,8},{16,20},{20,16},{24,28},{28,24},{1,5},{5... | collective-permute-start | bytes 147464 | tf_op jit(solution)/shard_map/ppermute | solution.py:339
  17.2 2.5 %copy-start = (bf16[256,2048]{1,0:T(8,128)(2,1)S(1)}, bf16[256,2048]{1,0:T(8,128)(2,1)}, u32[]{:S(2)}) copy-start(bf16[256,2048]{1,0:T(8,128)(2,1)} %wo_ref) | copy-start | bytes 3145732
  21.1 1.5 %collective-permute-start.6 = (bf16[48,2048]{1,0:T(8,128)(2,1)S(1)}, bf16[48,2048]{1,0:T(8,128)(2,1)S(1)}, u32[]{:S(2)}, u32[]{:S(2)}) collective-permute-start(bf16[48,2048]{1,0:T(8,128)(2,1)S(1)} %get-tuple-element.29), channel_id=1, source_target_pairs={{0,1},{1,0},{2,3},{3,2},{4,5},{5,4},{6,7},{7,6},{8,9},{9,8},{10,11... | collective-permute-start | bytes 589832 | tf_op jit(solution)/shard_map/ppermute | solution.py:370
  21.8 3.0 %collective-permute-start.5 = (bf16[48,2048]{1,0:T(8,128)(2,1)S(1)}, bf16[48,2048]{1,0:T(8,128)(2,1)S(1)}, u32[]{:S(2)}, u32[]{:S(2)}) collective-permute-start(bf16[48,2048]{1,0:T(8,128)(2,1)S(1)} %get-tuple-element.27), channel_id=1, source_target_pairs={{0,1},{1,0},{2,3},{3,2},{4,5},{5,4},{6,7},{7,6},{8,9},{9,8},{10,11... | collective-permute-start | bytes 589832 | tf_op jit(solution)/shard_map/ppermute | solution.py:370
  22.6 7.0 %collective-permute-start.7 = (bf16[48,2048]{1,0:T(8,128)(2,1)S(1)}, bf16[48,2048]{1,0:T(8,128)(2,1)S(1)}, u32[]{:S(2)}, u32[]{:S(2)}) collective-permute-start(bf16[48,2048]{1,0:T(8,128)(2,1)S(1)} %add_convert_fusion.1), channel_id=1, source_target_pairs={{0,2},{1,3},{2,0},{3,1},{4,6},{5,7},{6,4},{7,5},{8,10},{9,11},{10,... | collective-permute-start | bytes 589832 | tf_op jit(solution)/shard_map/ppermute | solution.py:370
